TPU v7x, 32 devices: a whole 2x2x4 slice. The times are simulated.
32 devices in a mesh: grp: 2 (over x), tp: 16 (over z, y, core).
Axes of the slice: x: 2, y: 2, z: 4, core: 2. Of those that a mesh axis runs over, the one named last changes fastest.
Arguments:
- residual_channel: bfloat16 [256, 8, 4096], P('grp', None, 'tp'), parts along dimension 0, may hold values from -18 to 18, as said below
- prior_block_multiplier: float32 [2, 4096], replicated, may hold values from 0.1 to 1.9
- probe_map_matrix: bfloat16 [2, 4096, 2048], P(None, None, 'tp'), may hold values from -0.09375 to 0.09375
- lookup_map_matrix: bfloat16 [2, 4096, 2048], P(None, None, 'tp'), may hold values from -0.09375 to 0.09375
- content_map_matrix: bfloat16 [2, 4096, 2048], P(None, None, 'tp'), may hold values from -0.09375 to 0.09375
- emission_valve_matrix: bfloat16 [2, 4096, 2048], P(None, None, 'tp'), may hold values from -0.09375 to 0.09375
- forgetting_map_matrix: bfloat16 [2, 4096, 32], replicated, may hold values from -0.09375 to 0.09375
- insertion_rate_matrix: bfloat16 [2, 4096, 32], replicated, may hold values from -0.09375 to 0.09375
- forgetting_magnitude_exponent: float32 [2, 32], P(None, 'tp'), may hold values from -4.6 to -1.2
- channel_forgetting_offset: float32 [2, 32], P(None, 'tp'), may hold values from -2 to 1
- surplus_forgetting_amounts: float32 [2, 256, 8, 32], P(None, 'grp', None, 'tp'), parts along dimension 1, may hold values from -0.7 to 0
- readout_rescale_multiplier: float32 [2, 2048], P(None, 'tp'), may hold values from 0.1 to 1.9
- emission_map_matrix: bfloat16 [2, 2048, 4096], P(None, None, 'tp'), may hold values from -2 to 2
- post_mixing_multiplier: float32 [2, 4096], replicated, may hold values from 0.1 to 1.9
- recurrent_matrices: float32 [2, 256, 32, 4096], P(None, 'grp', 'tp'), parts along dimension 1, may hold values from -6 to 6
Outputs:
- new_stream: bfloat16 [256, 8, 4096], P('grp', None, 'tp'), parts along dimension 0
- new_memory: float32 [2, 256, 32, 4096], P(None, 'grp', 'tp'), parts along dimension 1
There are 2 independent parts, one for each index of `grp`. A program takes and returns all parts, laid end to end along the dimension named above; an argument that names none is the same for every part. Nothing has to cross between parts.
Inputs may be any that keep to these rules, and one draw needn't show every extreme that they name: `residual_channel`: column scales of the features differ widely.
All inputs are finite; a program needn't handle non-finite values.
Results may differ from a plain program's by a relative error of at most 0.0081.
Values may be sent and summed in bfloat16 or wider, within the bound.
A program may use at most 192 MiB of HBM per device.

v0:
```python
import jax
import jax.numpy as jnp
from jax import lax
from jax.experimental import pallas as pl
from jax.experimental.pallas import tpu as pltpu
from jax.sharding import PartitionSpec as P

D = 4096
HEAD_DIM = 64
LAYERS = 2


EPS = 1e-06
HIGH = lax.Precision.HIGHEST


def solve_lower(a_mat, right_side):
    length = right_side.shape[-2]
    solved_rows = []
    for row_at in range(length):
        current_row = right_side[..., row_at, :]
        for col_at in range(row_at):
            current_row = current_row - a_mat[..., row_at, col_at][..., None] * solved_rows[col_at]
        solved_rows.append(current_row)
    return jnp.stack(solved_rows, axis=-2)


def delta_block(queries, key_rows, values, forgetting_exponent_amount, strength, matrix_state):
    length = queries.shape[2]
    causal = jnp.tril(jnp.ones((length, length), bool))
    strict = jnp.tril(jnp.ones((length, length), bool), -1)
    cumulative = jnp.cumsum(forgetting_exponent_amount, axis=-1)
    decay_mat = jnp.where(
        causal,
        jnp.exp(jnp.where(causal, cumulative[..., :, None] - cumulative[..., None, :], 0.0)),
        0.0,
    )
    key_gram = jnp.einsum("bhtd,bhsd->bhts", key_rows, key_rows, precision=HIGH)
    a_mat = jnp.where(strict, strength[..., :, None] * decay_mat * key_gram, 0.0)
    right_side = jnp.concatenate(
        [strength[..., None] * values, (strength * jnp.exp(cumulative))[..., None] * key_rows],
        axis=-1,
    )
    solved = solve_lower(a_mat, right_side)
    width_v = values.shape[-1]
    update = solved[..., :width_v] - jnp.einsum(
        "bhtk,bhkv->bhtv", solved[..., width_v:], matrix_state, precision=HIGH
    )
    scores = jnp.einsum("bhtd,bhsd->bhts", queries, key_rows, precision=HIGH) * decay_mat
    output = jnp.exp(cumulative)[..., None] * jnp.einsum(
        "bhtk,bhkv->bhtv", queries, matrix_state, precision=HIGH
    )
    output = output + jnp.einsum("bhts,bhsv->bhtv", scores, update, precision=HIGH)
    final_log = cumulative[..., -1:]
    revised_memory_matrix = jnp.exp(final_log)[..., None] * matrix_state + jnp.einsum(
        "bhsk,bhsv->bhkv",
        key_rows * jnp.exp(final_log - cumulative)[..., None],
        update,
        precision=HIGH,
    )
    return (output, revised_memory_matrix)


def unit_rows(matrix):
    return matrix * lax.rsqrt(jnp.sum(matrix * matrix, axis=-1, keepdims=True) + EPS)


def token_blender(
    mapped_token_vectors,
    magnitude_exponent,
    offset_terms_array,
    surplus_forgetting_exponent,
    multiplier_terms_array,
    incoming_memory_matrix,
    batch_total,
    generation_round_total,
):
    rounded = [
        lax.optimization_barrier(part_sum.astype(jnp.bfloat16)).astype(jnp.float32)
        for part_sum in mapped_token_vectors
    ]
    queries, keys_raw, values_raw, gate_raw, decay_pre, strength_pre = rounded
    head_count = incoming_memory_matrix.shape[1]

    def to_heads(matrix):
        return matrix.reshape(batch_total, generation_round_total, head_count, HEAD_DIM).transpose(
            0, 2, 1, 3
        )

    def per_head(matrix):
        return matrix.reshape(batch_total, generation_round_total, head_count).transpose(0, 2, 1)

    queries = unit_rows(jax.nn.silu(to_heads(queries))) * HEAD_DIM ** (-0.5)
    key_rows = unit_rows(jax.nn.silu(to_heads(keys_raw)))
    values = jax.nn.silu(to_heads(values_raw))
    forgetting_exponent_amount = -jnp.exp(magnitude_exponent)[None, :, None] * jax.nn.softplus(
        per_head(decay_pre) + offset_terms_array[None, :, None]
    )
    forgetting_exponent_amount = forgetting_exponent_amount + surplus_forgetting_exponent.transpose(
        0, 2, 1
    )
    strength = jax.nn.sigmoid(per_head(strength_pre))
    matrix_state = incoming_memory_matrix.reshape(batch_total, head_count, HEAD_DIM, HEAD_DIM)
    output, revised_memory_matrix = delta_block(
        queries, key_rows, values, forgetting_exponent_amount, strength, matrix_state
    )
    normed = output * lax.rsqrt(jnp.mean(output * output, axis=-1, keepdims=True) + EPS)
    normed = (
        normed
        * multiplier_terms_array.reshape(head_count, HEAD_DIM)[None, :, None, :]
        * jax.nn.silu(to_heads(gate_raw))
    )
    blended_token_vectors = (
        normed.transpose(0, 2, 1, 3)
        .reshape(batch_total * generation_round_total, head_count * HEAD_DIM)
        .astype(jnp.bfloat16)
    )
    return (
        blended_token_vectors,
        revised_memory_matrix.reshape(batch_total, head_count, HEAD_DIM * HEAD_DIM),
    )


LANES = 128


def bf16_dot(left, right):
    return jnp.dot(left, right, preferred_element_type=jnp.float32)


def head_sums(squares, ones):
    high = squares.astype(jnp.bfloat16)
    low = (squares - high.astype(jnp.float32)).astype(jnp.bfloat16)
    return bf16_dot(high, ones) + bf16_dot(low, ones)


def mixer_kernel(
    proj_ref, surplus_ref, vec_ref, spread_ref, ones_ref, perm_ref, state_ref, *rest
):
    y_ref, new_ref, qk_ref, x_ref, kd_ref, u_ref, qs_ref, dec_ref = rest[-8:]
    rows = proj_ref.shape[0]
    seqs, steps = qk_ref.shape[1], qk_ref.shape[2]
    f32, bf16 = jnp.float32, jnp.bfloat16
    ones = ones_ref[...]
    perm = perm_ref[...]

    def cols(at):
        return proj_ref[:, at * LANES : (at + 1) * LANES].astype(f32)

    def tokens(matrix):
        return matrix.reshape(seqs, steps, LANES)

    queries = jax.nn.silu(cols(0))
    keys = jax.nn.silu(cols(1))
    sums = head_sums(jnp.concatenate([queries * queries, keys * keys], axis=1), ones)
    queries = tokens(queries * lax.rsqrt(sums[:, :LANES] + EPS) * HEAD_DIM ** (-0.5))
    keys = tokens(keys * lax.rsqrt(sums[:, LANES:] + EPS))
    spread = bf16_dot(proj_ref[:, 4 * LANES : 5 * LANES], spread_ref[...])
    biased = spread[:, :LANES] + vec_ref[1:2, :]
    softplus = jnp.maximum(biased, 0.0) + jnp.log1p(jnp.exp(-jnp.abs(biased)))
    cumulative = tokens(vec_ref[0:1, :] * softplus + surplus_ref[...])
    beta = tokens(jax.nn.sigmoid(spread[:, LANES:]))
    token = lax.broadcasted_iota(jnp.int32, (seqs, steps, LANES), 1)
    shift = 1
    while shift < steps:
        moved = pltpu.roll(cumulative, shift, axis=1)
        cumulative = cumulative + jnp.where(token >= shift, moved, 0.0)
        shift *= 2
    grown = jnp.exp(cumulative)
    solved_u = beta * tokens(jax.nn.silu(cols(2)))
    solved_p = beta * grown * keys
    for at in range(steps):
        causal = token >= at
        gap = jnp.where(causal, cumulative - cumulative[:, at : at + 1, :], 0.0)
        decay = jnp.where(causal, jnp.exp(gap), 0.0)
        key_row = keys[:, at : at + 1, :]
        pair = jnp.concatenate([queries * key_row, keys * key_row], axis=2)
        dots = bf16_dot(pair.reshape(rows, 2 * LANES).astype(bf16), ones)
        qk_ref[at] = tokens(dots[:, :LANES]) * decay
        if at < steps - 1:
            a_col = jnp.where(token > at, beta * decay * tokens(dots[:, LANES:]), 0.0)
            solved_u = solved_u - a_col * solved_u[:, at : at + 1, :]
            solved_p = solved_p - a_col * solved_p[:, at : at + 1, :]
    last = cumulative[:, steps - 1 : steps, :]
    faded = keys * jnp.exp(last - cumulative)

    def permuted(first, second):
        both = jnp.concatenate([first, second], axis=1).reshape(2 * rows, LANES)
        return bf16_dot(both.astype(bf16), perm).astype(bf16).reshape(seqs, 2 * steps, LANES)

    x_ref[...] = permuted(queries, solved_p)
    kd_ref[...] = permuted(faded, faded)
    u_ref[...] = solved_u
    dec_ref[...] = jnp.broadcast_to(jnp.exp(last), (seqs, steps, LANES))

    state_rows = state_ref.shape[2]
    even = lax.broadcasted_iota(jnp.int32, (state_rows, LANES), 0) % 2 == 0
    left = lax.broadcasted_iota(jnp.int32, (state_rows, LANES), 1) < HEAD_DIM
    kept = even == left

    def one_sequence(at, carry):
        state = state_ref[0, at]
        turned = pltpu.roll(state, HEAD_DIM, axis=1)
        upper = jnp.where(kept, jnp.where(even, state, turned), 0.0)
        lower = jnp.where(kept, jnp.where(even, turned, state), 0.0)
        wide = jnp.concatenate([upper, lower], axis=0).astype(bf16)
        read = bf16_dot(x_ref[at], wide)
        qs_ref[at] = read[:steps]
        update = u_ref[at] - read[steps:]
        u_ref[at] = update
        high = update.astype(bf16).astype(f32)
        split = jnp.concatenate([high, update - high], axis=0).astype(bf16)
        grow = lax.dot_general(
            kd_ref[at], split, (((0,), (0,)), ((), ())), preferred_element_type=f32
        )
        grow_0, grow_1 = grow[:state_rows], grow[state_rows:]
        crossed = pltpu.roll(jnp.where(even, grow_1, grow_0), HEAD_DIM, axis=1)
        added = jnp.where(kept, jnp.where(even, grow_0, grow_1), crossed)
        fade = dec_ref[at]
        fade_turned = pltpu.roll(fade, HEAD_DIM, axis=1)
        copies = state_rows // steps
        factor = jnp.where(
            kept,
            jnp.concatenate([fade] * copies, axis=0),
            jnp.concatenate([fade_turned] * copies, axis=0),
        )
        new_ref[0, at] = factor * state + added
        return carry

    lax.fori_loop(0, seqs, one_sequence, 0, unroll=8)
    update = u_ref[...]
    output = grown * qs_ref[...]
    for at in range(steps):
        output = output + qk_ref[at] * update[:, at : at + 1, :]
    output = output.reshape(rows, LANES)
    squares = head_sums(output * output, ones[:LANES, :LANES])
    output = output * lax.rsqrt(squares * (1.0 / HEAD_DIM) + EPS)
    y_ref[...] = (output * vec_ref[2:3, :] * jax.nn.silu(cols(3))).astype(bf16)


def mixer_constants(head_count):
    row = jnp.arange(2 * LANES)[:, None]
    col = jnp.arange(2 * LANES)[None, :]
    ones = (row // HEAD_DIM == col // HEAD_DIM).astype(jnp.bfloat16)
    spread = (row[:LANES] == col // HEAD_DIM).astype(jnp.bfloat16)
    head, channel = row[:LANES] // HEAD_DIM, row[:LANES] % HEAD_DIM
    target = (channel % 2) * HEAD_DIM + (channel // 2) * head_count + head
    perm = (target == col[:, :LANES]).astype(jnp.bfloat16)
    return spread, ones, perm


def mixer(proj, surplus, vectors, constants, states, layer, earlier):
    rows = proj.shape[0]
    layers, all_seqs, state_rows, _ = states.shape
    seqs_here = all_seqs
    steps = rows // seqs_here
    block = next(size for size in (32, 16, 8, 4, 2, 1) if seqs_here % size == 0)
    token_rows = block * steps
    spread, ones, perm = constants

    def whole(array):
        return pl.BlockSpec(array.shape, lambda i: (0,) * array.ndim)

    in_specs = [
        pl.BlockSpec((token_rows, proj.shape[1]), lambda i: (i, 0)),
        pl.BlockSpec((token_rows, LANES), lambda i: (i, 0)),
        whole(vectors),
        whole(spread),
        whole(ones),
        whole(perm),
        pl.BlockSpec((1, block, state_rows, LANES), lambda i: (layer, i, 0, 0)),
    ]
    operands = [proj, surplus, vectors, spread, ones, perm, states]
    aliases = {}
    if earlier is not None:
        in_specs.append(pl.BlockSpec(memory_space=pl.ANY))
        operands.append(earlier)
        aliases = {len(operands) - 1: 1}
    tile = (block, steps, LANES)
    return pl.pallas_call(
        mixer_kernel,
        grid=(seqs_here // block,),
        in_specs=in_specs,
        out_specs=[
            pl.BlockSpec((token_rows, LANES), lambda i: (i, 0)),
            pl.BlockSpec((1, block, state_rows, LANES), lambda i: (layer, i, 0, 0)),
        ],
        out_shape=[
            jax.ShapeDtypeStruct((rows, LANES), jnp.bfloat16),
            jax.ShapeDtypeStruct(states.shape, jnp.float32),
        ],
        scratch_shapes=[
            pltpu.VMEM((steps,) + tile, jnp.float32),
            pltpu.VMEM((block, 2 * steps, LANES), jnp.bfloat16),
            pltpu.VMEM((block, 2 * steps, LANES), jnp.bfloat16),
            pltpu.VMEM(tile, jnp.float32),
            pltpu.VMEM(tile, jnp.float32),
            pltpu.VMEM(tile, jnp.float32),
        ],
        input_output_aliases=aliases,
        cost_estimate=pl.CostEstimate(
            flops=rows * 20 * 2 * LANES * 2 * LANES,
            bytes_accessed=2 * all_seqs * state_rows * LANES * 4,
            transcendentals=rows * LANES * 12,
        ),
        name="mixer",
    )(*operands)


def project(portion, weights):
    return tuple(
        (jnp.dot(portion, weight, preferred_element_type=jnp.float32) for weight in weights)
    )


def out_project(blended_token_vectors, weight_rows):
    return jnp.dot(
        lax.all_gather(blended_token_vectors, "tp", axis=1, tiled=True),
        weight_rows,
        preferred_element_type=jnp.float32,
    ).astype(jnp.bfloat16)


def post_residual(widened, mixed_out, multiplier_terms_array, complete):
    mixed_wide = lax.optimization_barrier(mixed_out).astype(jnp.float32)
    squares = jnp.sum(mixed_wide * mixed_wide, axis=-1)
    if not complete:
        squares = lax.psum(squares, "tp")
    post_rms = lax.rsqrt(squares / D + EPS)[:, None]
    return lax.optimization_barrier(
        (widened + mixed_wide * post_rms * multiplier_terms_array).astype(jnp.bfloat16)
    )


def local(
    residual_channel,
    prior_block_multiplier,
    probe_map_matrix,
    lookup_map_matrix,
    content_map_matrix,
    emission_valve_matrix,
    forgetting_map_matrix,
    insertion_rate_matrix,
    forgetting_magnitude_exponent,
    channel_forgetting_offset,
    surplus_forgetting_amounts,
    readout_rescale_multiplier,
    emission_map_matrix,
    post_mixing_multiplier,
    recurrent_matrices,
):
    batch_total, generation_round_total, own_width = residual_channel.shape
    head_count = recurrent_matrices.shape[2]
    row_count = batch_total * generation_round_total
    col_offset = lax.axis_index("tp") * own_width
    head_offset = lax.axis_index("tp") * head_count
    new_states = []

    def mix_layer(mapped_token_vectors, block_index_number):
        blended_token_vectors, revised_memory_matrix = token_blender(
            mapped_token_vectors,
            forgetting_magnitude_exponent[block_index_number],
            channel_forgetting_offset[block_index_number],
            surplus_forgetting_amounts[block_index_number],
            readout_rescale_multiplier[block_index_number],
            recurrent_matrices[block_index_number],
            batch_total,
            generation_round_total,
        )
        new_states.append(revised_memory_matrix)
        return out_project(blended_token_vectors, emission_map_matrix[block_index_number])

    def own_cols(matrix):
        return lax.dynamic_slice_in_dim(matrix, col_offset, own_width, matrix.ndim - 1)

    whole_rows = lax.all_gather(
        residual_channel.reshape(row_count, own_width), "tp", axis=1, tiled=True
    )
    current = whole_rows
    for block_index_number in range(LAYERS):
        widened = whole_rows.astype(jnp.float32)
        inv_rms = lax.rsqrt(jnp.mean(widened * widened, axis=-1, keepdims=True) + EPS)
        hidden = (widened * inv_rms * prior_block_multiplier[block_index_number]).astype(
            jnp.bfloat16
        )
        weights = (
            probe_map_matrix[block_index_number],
            lookup_map_matrix[block_index_number],
            content_map_matrix[block_index_number],
            emission_valve_matrix[block_index_number],
            lax.dynamic_slice_in_dim(
                forgetting_map_matrix[block_index_number], head_offset, head_count, 1
            ),
            lax.dynamic_slice_in_dim(
                insertion_rate_matrix[block_index_number], head_offset, head_count, 1
            ),
        )
        mapped_token_vectors = project(hidden, weights)
        mixed_out = mix_layer(mapped_token_vectors, block_index_number)
        if block_index_number < LAYERS - 1:
            gathered = lax.all_gather(mixed_out, "tp", axis=1, tiled=True)
            whole_rows = post_residual(
                widened, gathered, post_mixing_multiplier[block_index_number], True
            )
        else:
            current = post_residual(
                own_cols(widened),
                mixed_out,
                own_cols(post_mixing_multiplier[block_index_number]),
                False,
            )
    return (
        current.reshape(batch_total, generation_round_total, own_width),
        jnp.stack(new_states, axis=0),
    )


PARTS = 2


def gather_kernel(count, src_ref, out_ref, right_sem, left_sem, over_sem, twin_sem, land_sem, own_sem):
    me = lax.axis_index("tp")
    depth = count // 4
    core, row, line = lax.rem(me, 2), lax.rem(me // 2, 2), me // 4
    over, twin = me + 2 - 4 * row, me + 1 - 2 * core
    width = src_ref.shape[1]
    part_rows = src_ref.shape[0] // PARTS
    has_left, has_right = line > 0, line < depth - 1
    barrier = pltpu.get_barrier_semaphore()

    def greet(device):
        pl.semaphore_signal(
            barrier, inc=1, device_id={"tp": device}, device_id_type=pl.DeviceIdType.MESH
        )

    greet(over)
    greet(twin)

    greet(lax.rem(me + 4, count))
    greet(lax.rem(me + count - 4, count))
    pl.semaphore_wait(barrier, 4)

    def spot(origin, part):
        return out_ref.at[
            pl.ds(part * part_rows, part_rows), pl.ds(pl.multiple_of(origin * width, 128), width)
        ]

    def transfer(origin, part, device, send_sem, own):
        source = src_ref.at[pl.ds(part * part_rows, part_rows), :] if own else spot(origin, part)
        return pltpu.make_async_remote_copy(
            src_ref=source,
            dst_ref=spot(origin, part),
            send_sem=send_sem,
            recv_sem=land_sem.at[origin, part],
            device_id={"tp": device},
            device_id_type=pl.DeviceIdType.MESH,
        )

    ending = []

    def send(origin, part, device, send_sem, when, own=False):
        @pl.when(when)
        def _():
            transfer(origin, part, device, send_sem, own).start()

        def finish():
            @pl.when(when)
            def _():
                transfer(origin, part, device, send_sem, own).wait_send()

        ending.append(finish)

    def arrived(origin, part, when):
        @pl.when(when)
        def _():
            transfer(origin, part, twin, twin_sem.at[0, 0], False).wait_recv()

    always = line >= 0
    own_copies = []
    for part in range(PARTS):
        send(me, part, me + 4, right_sem.at[0, part], has_right, True)
        send(me, part, me - 4, left_sem.at[0, part], has_left, True)
        send(me, part, over, over_sem.at[0, part], always, True)
        send(me, part, twin, twin_sem.at[0, part], always, True)
        copy = pltpu.make_async_copy(
            src_ref.at[pl.ds(part * part_rows, part_rows), :], spot(me, part), own_sem.at[part]
        )
        copy.start()
        own_copies.append(copy)

    def crossing(hop):
        for part in range(PARTS):
            if hop == 0:
                arrived(over, part, always)
                send(over, part, twin, twin_sem.at[1, part], always)
            else:
                arrived(over - 4 * hop, part, line >= hop)
                send(over - 4 * hop, part, twin, twin_sem.at[4 * hop + 2, part], line >= hop)
                ahead = line + hop < depth
                arrived(over + 4 * hop, part, ahead)
                send(over + 4 * hop, part, twin, twin_sem.at[4 * hop + 3, part], ahead)

    for hop in range(1, depth):
        for part in range(PARTS):
            behind, ahead = line >= hop, line + hop < depth
            origin = me - 4 * hop
            arrived(origin, part, behind)
            if hop < depth - 1:
                send(origin, part, me + 4, right_sem.at[hop, part], behind & has_right)
            send(origin, part, over, over_sem.at[2 * hop, part], behind)
            send(origin, part, twin, twin_sem.at[4 * hop, part], behind)
            origin = me + 4 * hop
            arrived(origin, part, ahead)
            if hop < depth - 1:
                send(origin, part, me - 4, left_sem.at[hop, part], ahead & has_left)
            send(origin, part, over, over_sem.at[2 * hop + 1, part], ahead)
            send(origin, part, twin, twin_sem.at[4 * hop + 1, part], ahead)
        crossing(hop - 1)
    crossing(depth - 1)
    for place in range(count // 2):
        for part in range(PARTS):
            arrived(2 * place + 1 - core, part, always)
    for finish in ending:
        finish()
    for copy in own_copies:
        copy.wait()


def gather_columns(block, count, collective):
    rows, width = block.shape
    depth = count // 4
    dma = pltpu.SemaphoreType.DMA
    return pl.pallas_call(
        lambda *refs: gather_kernel(count, *refs),
        out_shape=jax.ShapeDtypeStruct((rows, count * width), block.dtype),
        in_specs=[pl.BlockSpec(memory_space=pltpu.VMEM)],
        out_specs=pl.BlockSpec(memory_space=pl.ANY),
        scratch_shapes=[
            dma((depth, PARTS)),
            dma((depth, PARTS)),
            dma((2 * depth, PARTS)),
            dma((4 * depth, PARTS)),
            dma((count, PARTS)),
            dma((PARTS,)),
        ],
        compiler_params=pltpu.CompilerParams(collective_id=collective, has_side_effects=True),
        cost_estimate=pl.CostEstimate(
            flops=0, bytes_accessed=count * rows * width * 2, transcendentals=0
        ),
        name="gather_columns",
    )(block)


def total_kernel(count, src_ref, out_ref, held_ref, send_sem, land_sem):
    me = lax.axis_index("tp")
    barrier = pltpu.get_barrier_semaphore()
    for step in range(1, count):
        pl.semaphore_signal(
            barrier,
            inc=1,
            device_id={"tp": lax.rem(me + step, count)},
            device_id_type=pl.DeviceIdType.MESH,
        )
    pl.semaphore_wait(barrier, count - 1)
    copies = []
    for step in range(1, count):
        copies.append(
            pltpu.make_async_remote_copy(
                src_ref=src_ref,
                dst_ref=held_ref.at[step],
                send_sem=send_sem.at[step],
                recv_sem=land_sem.at[step],
                device_id={"tp": lax.rem(me + step, count)},
                device_id_type=pl.DeviceIdType.MESH,
            )
        )
        copies[-1].start()
    total = src_ref[...]
    for step, copy in enumerate(copies):
        copy.wait_recv()
        total = total + held_ref[step + 1]
    out_ref[...] = total
    for copy in copies:
        copy.wait_send()


def total_over(sums, count, collective):
    tile = (sums.shape[0] // LANES, LANES)
    dma = pltpu.SemaphoreType.DMA
    total = pl.pallas_call(
        lambda *refs: total_kernel(count, *refs),
        out_shape=jax.ShapeDtypeStruct(tile, sums.dtype),
        in_specs=[pl.BlockSpec(memory_space=pltpu.VMEM)],
        out_specs=pl.BlockSpec(memory_space=pltpu.VMEM),
        scratch_shapes=[pltpu.VMEM((count,) + tile, sums.dtype), dma((count,)), dma((count,))],
        compiler_params=pltpu.CompilerParams(collective_id=collective, has_side_effects=True),
        name="total_over",
    )(sums.reshape(tile))
    return total.reshape(sums.shape)


def local_two_heads(
    residual_channel,
    prior_block_multiplier,
    probe_map_matrix,
    lookup_map_matrix,
    content_map_matrix,
    emission_valve_matrix,
    forgetting_map_matrix,
    insertion_rate_matrix,
    forgetting_magnitude_exponent,
    channel_forgetting_offset,
    surplus_forgetting_amounts,
    readout_rescale_multiplier,
    emission_map_matrix,
    post_mixing_multiplier,
    recurrent_matrices,
):
    batch_total, steps, own_width = residual_channel.shape
    layers, _, head_count, state_size = recurrent_matrices.shape
    row_count = batch_total * steps
    col_offset = lax.axis_index("tp") * own_width
    head_offset = lax.axis_index("tp") * head_count
    device_count = lax.axis_size("tp")

    def own_cols(matrix):
        return lax.dynamic_slice_in_dim(matrix, col_offset, own_width, matrix.ndim - 1)

    whole_rows = lax.all_gather(
        residual_channel.reshape(row_count, own_width), "tp", axis=1, tiled=True
    )
    constants = mixer_constants(head_count)
    groups = state_size // LANES
    states = (
        recurrent_matrices.reshape(layers, batch_total, head_count, groups, LANES)
        .transpose(0, 1, 3, 2, 4)
        .reshape(layers, batch_total, groups * head_count, LANES)
    )
    rates = [
        lax.dynamic_slice_in_dim(matrix, head_offset, head_count, 2)
        for matrix in (forgetting_map_matrix, insertion_rate_matrix)
    ]
    filler = jnp.zeros(rates[0].shape[:2] + (LANES - 2 * head_count,), jnp.bfloat16)
    weights = [
        jnp.concatenate(
            [
                matrix[layer]
                for matrix in (
                    probe_map_matrix,
                    lookup_map_matrix,
                    content_map_matrix,
                    emission_valve_matrix,
                    rates[0],
                    rates[1],
                    filler,
                )
            ],
            axis=1,
        )
        for layer in range(layers)
    ]
    surplus = jnp.repeat(
        surplus_forgetting_amounts.reshape(layers, row_count, head_count), HEAD_DIM, axis=2
    )
    vectors = jnp.stack(
        [
            jnp.repeat(-jnp.exp(forgetting_magnitude_exponent), HEAD_DIM, axis=1),
            jnp.repeat(channel_forgetting_offset, HEAD_DIM, axis=1),
            readout_rescale_multiplier,
        ],
        axis=1,
    )
    earlier = None
    current = None
    for layer in range(layers):
        widened = whole_rows.astype(jnp.float32)
        inv_rms = lax.rsqrt(jnp.mean(widened * widened, axis=-1, keepdims=True) + EPS)
        hidden = (widened * inv_rms * prior_block_multiplier[layer]).astype(jnp.bfloat16)
        proj = jnp.dot(hidden, weights[layer], preferred_element_type=jnp.float32).astype(
            jnp.bfloat16
        )
        readout, earlier = mixer(
            proj, surplus[layer], vectors[layer], constants, states, layer, earlier
        )
        spread_out = gather_columns(readout, device_count, 2 * layer + 1)
        mixed_out = jnp.dot(
            spread_out, emission_map_matrix[layer], preferred_element_type=jnp.float32
        ).astype(jnp.bfloat16)
        if layer < layers - 1:
            gathered = gather_columns(mixed_out, device_count, 2 * layer + 2)
            whole_rows = post_residual(widened, gathered, post_mixing_multiplier[layer], True)
        else:
            mixed_wide = lax.optimization_barrier(mixed_out).astype(jnp.float32)
            squares = total_over(
                jnp.sum(mixed_wide * mixed_wide, axis=-1), device_count, 2 * layer + 2
            )
            post_rms = lax.rsqrt(squares / D + EPS)[:, None]
            current = (
                own_cols(whole_rows).astype(jnp.float32)
                + mixed_wide * post_rms * own_cols(post_mixing_multiplier[layer])
            ).astype(jnp.bfloat16)
    new_memory = (
        earlier.reshape(layers, batch_total, groups, head_count, LANES)
        .transpose(0, 1, 3, 2, 4)
        .reshape(recurrent_matrices.shape)
    )
    return current.reshape(batch_total, steps, own_width), new_memory


def local_any(*arrays):
    residual_channel, recurrent_matrices = arrays[0], arrays[-1]
    two_heads = (
        recurrent_matrices.shape[2] * HEAD_DIM == LANES
        and residual_channel.shape[1] == 8
        and residual_channel.shape[0] % 16 == 0
        and residual_channel.shape[2] % LANES == 0
        and lax.axis_size("tp") % 4 == 0
        and lax.axis_size("tp") > 4
    )
    return (local_two_heads if two_heads else local)(*arrays)


def solution(mesh):
    return jax.shard_map(
        local_any,
        mesh=mesh,
        in_specs=(
            P("grp", None, "tp"),
            P(),
            P(None, None, "tp"),
            P(None, None, "tp"),
            P(None, None, "tp"),
            P(None, None, "tp"),
            P(),
            P(),
            P(None, "tp"),
            P(None, "tp"),
            P(None, "grp", None, "tp"),
            P(None, "tp"),
            P(None, None, "tp"),
            P(),
            P(None, "grp", "tp", None),
        ),
        out_specs=(P("grp", None, "tp"), P(None, "grp", "tp", None)),
        check_vma=False,
    )
```

profile of v0, /device:TPU:0, one launch (start us, length us, event | category | flops | bytes accessed | tf_op | source)
XLA Modules:
  0.0 327.5 jit_solution(6341260754560198880)
XLA Ops:
  7.2 0.0 all-gather.2.cloned.1.call-start
  7.2 0.7 all-gather.2.cloned.1.call-update
  7.9 1.0 dynamic-slice_bitcast_fusion.2
  8.9 1.4 copy.29
  10.3 1.4 copy.30
  11.7 0.5 copy.24
  12.3 0.5 copy.25
  12.8 0.7 fusion.40
  13.5 0.1 copy.26
  13.6 0.1 slice.100
  13.8 1.0 copy.28.surplus_ref
  14.8 0.7 broadcast_in_dim.25
  15.5 0.1 stack_reshape.7
  15.6 0.7 exponential_negate_fusion
  16.3 0.1 broadcast_in_dim.24
  16.4 0.1 stack_reshape.6
  16.5 0.1 copy.31
  16.6 0.1 slice.114
  16.8 1.0 copy.32.surplus_ref
  17.8 0.0 copy-start.3
  17.8 0.0 copy-start.4
  17.8 4.5 %slice_bitcast_fusion.6 = (bf16[4096,128]{1,0:T(8,128)(2,1)}, bf16[4096,128]{1,0:T(8,128)(2,1)}, bf16[4096,128]{1,0:T(8,128)(2,1)}, bf16[4096,128]{1,0:T(8,128)(2,1)}) fusion(bf16[2,4096,128]{2,1,0:T(8,128)(2,1)} %param.18, bf16[2,4096,128]{2,1,0:T(8,128)(2,1)} %param.17), kind=kLoop, calls=%fused_computation.42 | loop fusion | bytes 8388608 | tf_op jit(solution)/shard_map/squeeze | solution.py:647
  22.3 0.0 copy-done.3
  22.3 0.1 copy-done.4
  22.3 2.1 slice_bitcast_fusion.4
  24.4 0.1 broadcast.158
  24.6 10.2 %concatenate.7 = bf16[4096,640]{1,0:T(8,128)(2,1)} concatenate(bf16[4096,128]{1,0:T(8,128)(2,1)} %get-tuple-element.34, bf16[4096,128]{1,0:T(8,128)(2,1)} %get-tuple-element.15, bf16[4096,128]{1,0:T(8,128)(2,1)} %get-tuple-element.32, bf16[4096,128]{1,0:T(8,128)(2,1)} %get-tuple-element.11, bf16[4096,2]{1,0:T(8,128)(2,1)} %copy.29, bf16[4096,2]{1,0:T(8,128)(2,1)} %copy.30, ...), dimensions={1} | concatenate | bytes 10485760 | tf_op jit(solution)/shard_map/concatenate | solution.py:645
  34.8 0.0 copy-start.6
  34.8 9.9 %concatenate.6 = bf16[4096,640]{1,0:T(8,128)(2,1)} concatenate(bf16[4096,128]{1,0:T(8,128)(2,1)} %get-tuple-element.35, bf16[4096,128]{1,0:T(8,128)(2,1)} %get-tuple-element.14, bf16[4096,128]{1,0:T(8,128)(2,1)} %get-tuple-element.33, bf16[4096,128]{1,0:T(8,128)(2,1)} %get-tuple-element.10, bf16[4096,2]{1,0:T(8,128)(2,1)S(1)} %copy.24, bf16[4096,2]{1,0:T(8,128)(2,1)S(1)} %copy.25, ...), dimensions={1} | concatenate | bytes 10485760 | tf_op jit(solution)/shard_map/concatenate | solution.py:645
  44.7 0.0 copy-done.5
  44.8 0.0 copy-done.7
  44.8 0.6 slice_bitcast_fusion.8
  45.4 0.7 compare_convert_fusion.2.perm_ref
  46.1 0.7 compare_convert_fusion.1.spread_ref
  46.8 0.8 compare_convert_fusion.ones_ref
  47.6 0.0 copy-done.6
  47.6 43.0 %all-gather.2.cloned.1.call-done = bf16[1024,4096]{1,0:T(8,128)(2,1)} async-done(((bf16[1024,256]{1,0:T(8,128)(2,1)}), bf16[1024,4096]{1,0:T(8,128)(2,1)}) %all-gather.2.cloned.1.call-update) | async-done | bytes 8388624 | tf_op jit(solution)/shard_map/all_gather | solution.py:629
  90.6 5.2 %fusion.5 = f32[1024]{0:T(1024)S(1)} fusion(bf16[1024,4096]{1,0:T(8,128)(2,1)} %all-gather.2.cloned.1.call-done), kind=kLoop, calls=%fused_computation.12 | loop fusion | flops 12581888 | bytes 8392704 | tf_op jit(solution)/shard_map/reduce_sum | solution.py:677
  95.8 0.5 copy-done.2
  96.4 10.4 %fusion.20.proj_ref = bf16[1024,640]{1,0:T(8,128)(2,1)} fusion(bf16[4096,640]{1,0:T(8,128)(2,1)} %concatenate.6, bf16[1024,4096]{1,0:T(8,128)(2,1)S(1)} %copy-done.2, f32[4096]{0:T(1024)S(1)} %bitcast.86, f32[1024]{0:T(1024)S(1)} %add_rsqrt_fusion.2), kind=kOutput, calls=%fused_computation.23 | convolution fusion | flops 5386141696 | bytes 14962688 | tf_op jit(solution)/shard_map/dot_general | solution.py:679
  106.8 30.5 %mixer.2 = (bf16[1024,128]{1,0:T(8,128)(2,1)}, f32[2,128,64,128]{3,2,1,0:T(8,128)}) custom-call(bf16[1024,640]{1,0:T(8,128)(2,1)} %fusion.20.proj_ref, f32[1024,128]{1,0:T(8,128)} %copy.28.surplus_ref, f32[3,128]{1,0:T(4,128)} %get-tuple-element.29.vec_ref, bf16[128,256]{1,0:T(8,128)(2,1)} %compare_convert_fusion.1.spread_ref, ...), custom_call_target="tpu_custom_call" | custom-call | flops 1342177280 | bytes 8388608 | tf_op jit(solution)/shard_map/mixer/pallas_call | solution.py:280
  137.3 28.6 %gather_columns.3 = bf16[1024,2048]{1,0:T(8,128)(2,1)} custom-call(bf16[1024,128]{1,0:T(8,128)(2,1)} %get-tuple-element.6.refs_0_), custom_call_target="tpu_custom_call" | custom-call | bytes 4194304 | tf_op jit(solution)/shard_map/gather_columns/pallas_call | solution.py:533
  165.9 0.0 copy-done.8
  165.9 4.2 %convolution_convert_fusion.1.refs_0_ = bf16[1024,256]{1,0:T(8,128)(2,1)} fusion(bf16[1024,2048]{1,0:T(8,128)(2,1)} %gather_columns.3, bf16[2,2048,256]{2,1,0:T(8,128)(2,1)S(1)} %copy-done.8), kind=kOutput, calls=%fused_computation.27 | convolution fusion | flops 1074003968 | bytes 5767168 | tf_op jit(solution)/shard_map/dot_general | solution.py:686
  170.1 53.3 %gather_columns.4 = bf16[1024,4096]{1,0:T(8,128)(2,1)} custom-call(bf16[1024,256]{1,0:T(8,128)(2,1)} %convolution_convert_fusion.1.refs_0_), custom_call_target="tpu_custom_call" | custom-call | bytes 8388608 | tf_op jit(solution)/shard_map/gather_columns/pallas_call | solution.py:533
  223.4 0.0 copy-start
  223.4 0.0 slice-start
  223.5 5.2 %fusion = f32[1024]{0:T(1024)S(1)} fusion(bf16[1024,4096]{1,0:T(8,128)(2,1)} %gather_columns.4), kind=kLoop, calls=%fused_computation.7 | loop fusion | flops 12581888 | bytes 8392704 | tf_op jit(solution)/shard_map/reduce_sum | solution.py:326
  228.7 0.5 copy-done
  229.2 6.9 %fusion.8 = bf16[1024,4096]{1,0:T(8,128)(2,1)S(1)} fusion(bf16[1024,4096]{1,0:T(8,128)(2,1)S(1)} %copy-done, bf16[1024,4096]{1,0:T(8,128)(2,1)} %all-gather.2.cloned.1.call-done, f32[4096]{0:T(1024)S(1)} %bitcast.83, f32[1024]{0:T(1024)S(1)} %add_rsqrt_fusion.1), kind=kLoop, calls=%fused_computation.15 | loop fusion | flops 25165824 | bytes 25186304 | tf_op jit(solution)/shard_map/convert_element_type | solution.py:331
  236.2 0.0 copy-start.1
  236.2 1.7 fusion.2
  237.9 0.0 slice-done
  237.9 0.0 slice-done.1
  237.9 7.9 %fusion.17.proj_ref = bf16[1024,640]{1,0:T(8,128)(2,1)} fusion(bf16[4096,640]{1,0:T(8,128)(2,1)S(1)} %bitcast.79, bf16[1024,4096]{1,0:T(8,128)(2,1)S(1)} %fusion.8, f32[4096]{0:T(1024)S(1)} %bitcast.85, f32[1024]{0:T(1024)S(1)} %add_rsqrt_fusion), kind=kOutput, calls=%fused_computation.22 | convolution fusion | flops 5386141696 | bytes 14962688 | tf_op jit(solution)/shard_map/dot_general | solution.py:679
  245.8 0.0 copy-done.1
  245.8 30.7 %mixer.3 = (bf16[1024,128]{1,0:T(8,128)(2,1)}, f32[2,128,64,128]{3,2,1,0:T(8,128)}) custom-call(bf16[1024,640]{1,0:T(8,128)(2,1)} %fusion.17.proj_ref, f32[1024,128]{1,0:T(8,128)} %copy.32.surplus_ref, f32[3,128]{1,0:T(4,128)} %get-tuple-element.28.vec_ref, bf16[128,256]{1,0:T(8,128)(2,1)} %compare_convert_fusion.1.spread_ref, ...), custom_call_target="tpu_custom_call", output_to_operand_aliasing={{1}: (7, {})} | custom-call | flops 1342177280 | bytes 8388608 | tf_op jit(solution)/shard_map/mixer/pallas_call | solution.py:280
  276.5 28.8 %gather_columns.5 = bf16[1024,2048]{1,0:T(8,128)(2,1)} custom-call(bf16[1024,128]{1,0:T(8,128)(2,1)} %get-tuple-element.8.refs_0_), custom_call_target="tpu_custom_call" | custom-call | bytes 4194304 | tf_op jit(solution)/shard_map/gather_columns/pallas_call | solution.py:533
  305.3 0.0 copy-done.9
  305.3 3.4 %convolution_convert_fusion = bf16[1024,256]{1,0:T(8,128)(2,1)S(1)} fusion(bf16[1024,2048]{1,0:T(8,128)(2,1)} %gather_columns.5, bf16[2,2048,256]{2,1,0:T(8,128)(2,1)S(1)} %copy-done.9), kind=kOutput, calls=%fused_computation.26 | convolution fusion | flops 1074003968 | bytes 5767168 | tf_op jit(solution)/shard_map/dot_general | solution.py:686
  308.8 0.8 fusion.23
  309.6 8.3 %total_over.1 = f32[8,128]{1,0:T(8,128)} custom-call(f32[8,128]{1,0:T(8,128)} %bitcast.84), custom_call_target="tpu_custom_call" | custom-call | tf_op jit(solution)/shard_map/total_over/pallas_call | solution.py:590
  317.9 0.7 rsqrt_bitcast_fusion
  318.6 2.1 fusion.31
  (20 shorter events, 0.2 us)
Async XLA Ops:
  7.2 83.4 %all-gather.2.cloned.1.call-start = ((), (), s32[]{:S(2)}) async-start(), calls=%async_computation | async-start | bytes 8912896 | tf_op jit(solution)/shard_map/all_gather | solution.py:629
  17.8 4.5 %copy-start.3 = (bf16[2,4096,128]{2,1,0:T(8,128)(2,1)S(1)}, bf16[2,4096,128]{2,1,0:T(8,128)(2,1)}, u32[]{:S(2)}) copy-start(bf16[2,4096,128]{2,1,0:T(8,128)(2,1)} %param.20) | copy-start | bytes 6291460
  17.8 4.5 %copy-start.4 = (bf16[2,4096,128]{2,1,0:T(8,128)(2,1)S(1)}, bf16[2,4096,128]{2,1,0:T(8,128)(2,1)}, u32[]{:S(2)}) copy-start(bf16[2,4096,128]{2,1,0:T(8,128)(2,1)} %param.19) | copy-start | bytes 6291460
  34.8 10.0 %copy-start.5 = (f32[2,4096]{1,0:T(2,128)S(1)}, f32[2,4096]{1,0:T(2,128)}, u32[]{:S(2)}) copy-start(f32[2,4096]{1,0:T(2,128)} %param.28) | copy-start | bytes 98308
  34.8 10.0 %copy-start.7 = (f32[2,128]{1,0:T(2,128)S(1)}, f32[2,128]{1,0:T(2,128)}, u32[]{:S(2)}) copy-start(f32[2,128]{1,0:T(2,128)} %param.26) | copy-start | bytes 3076
  34.8 12.8 %copy-start.6 = (f32[2,4096]{1,0:T(2,128)S(1)}, f32[2,4096]{1,0:T(2,128)}, u32[]{:S(2)}) copy-start(f32[2,4096]{1,0:T(2,128)} %param.16) | copy-start | bytes 98308
  90.6 5.8 %copy-start.2 = (bf16[1024,4096]{1,0:T(8,128)(2,1)S(1)}, bf16[1024,4096]{1,0:T(8,128)(2,1)}, u32[]{:S(2)}) copy-start(bf16[1024,4096]{1,0:T(8,128)(2,1)} %all-gather.2.cloned.1.call-done) | copy-start | bytes 25165828
  106.8 59.1 %copy-start.8 = (bf16[2,2048,256]{2,1,0:T(8,128)(2,1)S(1)}, bf16[2,2048,256]{2,1,0:T(8,128)(2,1)}, u32[]{:S(2)}) copy-start(bf16[2,2048,256]{2,1,0:T(8,128)(2,1)} %param.27) | copy-start | bytes 6291460
  223.4 5.8 %copy-start = (bf16[1024,4096]{1,0:T(8,128)(2,1)S(1)}, bf16[1024,4096]{1,0:T(8,128)(2,1)}, u32[]{:S(2)}) copy-start(bf16[1024,4096]{1,0:T(8,128)(2,1)} %gather_columns.4) | copy-start | bytes 25165828
  223.4 14.4 %slice-start = ((s8[5242880]{0:T(1024)(128)(4,1)}), s8[4194304]{0:T(1024)(128)(4,1)S(1)}, s32[]{:S(2)}) async-start(s8[5242880]{0:T(1024)(128)(4,1)} %bitcast.78), calls=%async_computation.1 | async-start | bytes 8388608
  229.2 8.7 %slice-start.1 = ((s8[5242880]{0:T(1024)(128)(4,1)}), s8[1048576]{0:T(1024)(128)(4,1)S(1)}, s32[]{:S(2)}) async-start(s8[5242880]{0:T(1024)(128)(4,1)} %bitcast.78), calls=%async_computation.2 | async-start | bytes 2097152
  236.2 9.7 %copy-start.1 = (bf16[1024,4096]{1,0:T(8,128)(2,1)}, bf16[1024,4096]{1,0:T(8,128)(2,1)S(1)}, u32[]{:S(2)}) copy-start(bf16[1024,4096]{1,0:T(8,128)(2,1)S(1)} %fusion.8) | copy-start | bytes 25165828
  245.8 59.5 %copy-start.9 = (bf16[2,2048,256]{2,1,0:T(8,128)(2,1)S(1)}, bf16[2,2048,256]{2,1,0:T(8,128)(2,1)}, u32[]{:S(2)}) copy-start(bf16[2,2048,256]{2,1,0:T(8,128)(2,1)} %param.27) | copy-start | bytes 6291460
Sparse Core Ops, SparseCore 0:
  10.1 80.4 all-gather.1
where the time goes:
time: 329 us; the launch traced here: 328 us
  Pallas kernels  180 us (55%)
  waiting for transfers between devices  43.7 us (13%)
  local copies, waits for them, and re-layouts  37.8 us (11%)
  matrix products  26 us (8%)
  other arithmetic  25.6 us (8%)
  between operations  14.3 us (4%)
    pallas_call x3, Pallas kernels, gather_columns(): pl.pallas_call(lambda *refs: gather_kernel(count, *refs), out_shape=jax.S...  111 us
    pallas_call x2, Pallas kernels, mixer(): pl.pallas_call(mixer_kernel, grid=(seqs_here // block,), in_specs=in_spec...  61.2 us
    all_gather x1, waiting for transfers between devices, local_two_heads(): lax.all_gather(residual_channel.reshape(row_count, own_width), 'tp', axis...  43 us
    concatenate x2, local copies, waits for them, and re-layouts, local_two_heads(): jnp.concatenate([matrix[layer] for matrix in (probe_map_matrix, lookup_ma...  20.1 us
    dot_general x2, matrix products, local_two_heads(): jnp.dot(hidden, weights[layer], preferred_element_type=jnp.float32)  18.3 us
    squeeze x7, local copies, waits for them, and re-layouts, local_two_heads(): matrix[layer]  11.4 us
    pallas_call x1, Pallas kernels, total_over(): pl.pallas_call(lambda *refs: total_kernel(count, *refs), out_shape=jax.Sh...  8.3 us
    dot_general x2, matrix products, local_two_heads(): jnp.dot(spread_out, emission_map_matrix[layer], preferred_element_type=jn...  7.66 us
  transfers between devices with their start and end apart: 1, of which 1 were waited for; matrix products, arithmetic and copies ran while one was open for 12% of the time, Pallas kernels for 0%

commit v1 on v0

v1 whole, which is shorter than its diff:
```python
import jax
import jax.numpy as jnp
from jax import lax
from jax.experimental import pallas as pl
from jax.experimental.pallas import tpu as pltpu
from jax.sharding import PartitionSpec as P

D = 4096
HEAD_DIM = 64
LAYERS = 2


EPS = 1e-06
HIGH = lax.Precision.HIGHEST


def solve_lower(a_mat, right_side):
    length = right_side.shape[-2]
    solved_rows = []
    for row_at in range(length):
        current_row = right_side[..., row_at, :]
        for col_at in range(row_at):
            current_row = current_row - a_mat[..., row_at, col_at][..., None] * solved_rows[col_at]
        solved_rows.append(current_row)
    return jnp.stack(solved_rows, axis=-2)


def delta_block(queries, key_rows, values, forgetting_exponent_amount, strength, matrix_state):
    length = queries.shape[2]
    causal = jnp.tril(jnp.ones((length, length), bool))
    strict = jnp.tril(jnp.ones((length, length), bool), -1)
    cumulative = jnp.cumsum(forgetting_exponent_amount, axis=-1)
    decay_mat = jnp.where(
        causal,
        jnp.exp(jnp.where(causal, cumulative[..., :, None] - cumulative[..., None, :], 0.0)),
        0.0,
    )
    key_gram = jnp.einsum("bhtd,bhsd->bhts", key_rows, key_rows, precision=HIGH)
    a_mat = jnp.where(strict, strength[..., :, None] * decay_mat * key_gram, 0.0)
    right_side = jnp.concatenate(
        [strength[..., None] * values, (strength * jnp.exp(cumulative))[..., None] * key_rows],
        axis=-1,
    )
    solved = solve_lower(a_mat, right_side)
    width_v = values.shape[-1]
    update = solved[..., :width_v] - jnp.einsum(
        "bhtk,bhkv->bhtv", solved[..., width_v:], matrix_state, precision=HIGH
    )
    scores = jnp.einsum("bhtd,bhsd->bhts", queries, key_rows, precision=HIGH) * decay_mat
    output = jnp.exp(cumulative)[..., None] * jnp.einsum(
        "bhtk,bhkv->bhtv", queries, matrix_state, precision=HIGH
    )
    output = output + jnp.einsum("bhts,bhsv->bhtv", scores, update, precision=HIGH)
    final_log = cumulative[..., -1:]
    revised_memory_matrix = jnp.exp(final_log)[..., None] * matrix_state + jnp.einsum(
        "bhsk,bhsv->bhkv",
        key_rows * jnp.exp(final_log - cumulative)[..., None],
        update,
        precision=HIGH,
    )
    return (output, revised_memory_matrix)


def unit_rows(matrix):
    return matrix * lax.rsqrt(jnp.sum(matrix * matrix, axis=-1, keepdims=True) + EPS)


def token_blender(
    mapped_token_vectors,
    magnitude_exponent,
    offset_terms_array,
    surplus_forgetting_exponent,
    multiplier_terms_array,
    incoming_memory_matrix,
    batch_total,
    generation_round_total,
):
    rounded = [
        lax.optimization_barrier(part_sum.astype(jnp.bfloat16)).astype(jnp.float32)
        for part_sum in mapped_token_vectors
    ]
    queries, keys_raw, values_raw, gate_raw, decay_pre, strength_pre = rounded
    head_count = incoming_memory_matrix.shape[1]

    def to_heads(matrix):
        return matrix.reshape(batch_total, generation_round_total, head_count, HEAD_DIM).transpose(
            0, 2, 1, 3
        )

    def per_head(matrix):
        return matrix.reshape(batch_total, generation_round_total, head_count).transpose(0, 2, 1)

    queries = unit_rows(jax.nn.silu(to_heads(queries))) * HEAD_DIM ** (-0.5)
    key_rows = unit_rows(jax.nn.silu(to_heads(keys_raw)))
    values = jax.nn.silu(to_heads(values_raw))
    forgetting_exponent_amount = -jnp.exp(magnitude_exponent)[None, :, None] * jax.nn.softplus(
        per_head(decay_pre) + offset_terms_array[None, :, None]
    )
    forgetting_exponent_amount = forgetting_exponent_amount + surplus_forgetting_exponent.transpose(
        0, 2, 1
    )
    strength = jax.nn.sigmoid(per_head(strength_pre))
    matrix_state = incoming_memory_matrix.reshape(batch_total, head_count, HEAD_DIM, HEAD_DIM)
    output, revised_memory_matrix = delta_block(
        queries, key_rows, values, forgetting_exponent_amount, strength, matrix_state
    )
    normed = output * lax.rsqrt(jnp.mean(output * output, axis=-1, keepdims=True) + EPS)
    normed = (
        normed
        * multiplier_terms_array.reshape(head_count, HEAD_DIM)[None, :, None, :]
        * jax.nn.silu(to_heads(gate_raw))
    )
    blended_token_vectors = (
        normed.transpose(0, 2, 1, 3)
        .reshape(batch_total * generation_round_total, head_count * HEAD_DIM)
        .astype(jnp.bfloat16)
    )
    return (
        blended_token_vectors,
        revised_memory_matrix.reshape(batch_total, head_count, HEAD_DIM * HEAD_DIM),
    )


LANES = 128


def bf16_dot(left, right):
    return jnp.dot(left, right, preferred_element_type=jnp.float32)


def head_sums(squares, ones):
    high = squares.astype(jnp.bfloat16)
    low = (squares - high.astype(jnp.float32)).astype(jnp.bfloat16)
    return bf16_dot(high, ones) + bf16_dot(low, ones)


def project(portion, weights):
    return tuple(
        (jnp.dot(portion, weight, preferred_element_type=jnp.float32) for weight in weights)
    )


def out_project(blended_token_vectors, weight_rows):
    return jnp.dot(
        lax.all_gather(blended_token_vectors, "tp", axis=1, tiled=True),
        weight_rows,
        preferred_element_type=jnp.float32,
    ).astype(jnp.bfloat16)


def post_residual(widened, mixed_out, multiplier_terms_array, complete):
    mixed_wide = lax.optimization_barrier(mixed_out).astype(jnp.float32)
    squares = jnp.sum(mixed_wide * mixed_wide, axis=-1)
    if not complete:
        squares = lax.psum(squares, "tp")
    post_rms = lax.rsqrt(squares / D + EPS)[:, None]
    return lax.optimization_barrier(
        (widened + mixed_wide * post_rms * multiplier_terms_array).astype(jnp.bfloat16)
    )


def local(
    residual_channel,
    prior_block_multiplier,
    probe_map_matrix,
    lookup_map_matrix,
    content_map_matrix,
    emission_valve_matrix,
    forgetting_map_matrix,
    insertion_rate_matrix,
    forgetting_magnitude_exponent,
    channel_forgetting_offset,
    surplus_forgetting_amounts,
    readout_rescale_multiplier,
    emission_map_matrix,
    post_mixing_multiplier,
    recurrent_matrices,
):
    batch_total, generation_round_total, own_width = residual_channel.shape
    head_count = recurrent_matrices.shape[2]
    row_count = batch_total * generation_round_total
    col_offset = lax.axis_index("tp") * own_width
    head_offset = lax.axis_index("tp") * head_count
    new_states = []

    def mix_layer(mapped_token_vectors, block_index_number):
        blended_token_vectors, revised_memory_matrix = token_blender(
            mapped_token_vectors,
            forgetting_magnitude_exponent[block_index_number],
            channel_forgetting_offset[block_index_number],
            surplus_forgetting_amounts[block_index_number],
            readout_rescale_multiplier[block_index_number],
            recurrent_matrices[block_index_number],
            batch_total,
            generation_round_total,
        )
        new_states.append(revised_memory_matrix)
        return out_project(blended_token_vectors, emission_map_matrix[block_index_number])

    def own_cols(matrix):
        return lax.dynamic_slice_in_dim(matrix, col_offset, own_width, matrix.ndim - 1)

    whole_rows = lax.all_gather(
        residual_channel.reshape(row_count, own_width), "tp", axis=1, tiled=True
    )
    current = whole_rows
    for block_index_number in range(LAYERS):
        widened = whole_rows.astype(jnp.float32)
        inv_rms = lax.rsqrt(jnp.mean(widened * widened, axis=-1, keepdims=True) + EPS)
        hidden = (widened * inv_rms * prior_block_multiplier[block_index_number]).astype(
            jnp.bfloat16
        )
        weights = (
            probe_map_matrix[block_index_number],
            lookup_map_matrix[block_index_number],
            content_map_matrix[block_index_number],
            emission_valve_matrix[block_index_number],
            lax.dynamic_slice_in_dim(
                forgetting_map_matrix[block_index_number], head_offset, head_count, 1
            ),
            lax.dynamic_slice_in_dim(
                insertion_rate_matrix[block_index_number], head_offset, head_count, 1
            ),
        )
        mapped_token_vectors = project(hidden, weights)
        mixed_out = mix_layer(mapped_token_vectors, block_index_number)
        if block_index_number < LAYERS - 1:
            gathered = lax.all_gather(mixed_out, "tp", axis=1, tiled=True)
            whole_rows = post_residual(
                widened, gathered, post_mixing_multiplier[block_index_number], True
            )
        else:
            current = post_residual(
                own_cols(widened),
                mixed_out,
                own_cols(post_mixing_multiplier[block_index_number]),
                False,
            )
    return (
        current.reshape(batch_total, generation_round_total, own_width),
        jnp.stack(new_states, axis=0),
    )


CHUNKS = 4
GROUP_ROWS = 64


def step_kernel(
    count,
    chunks,
    x_hbm,
    probe_hbm,
    lookup_hbm,
    content_hbm,
    valve_hbm,
    forget_hbm,
    insert_hbm,
    emission_hbm,
    states_hbm,
    surplus_ref,
    pre_gain_ref,
    post_gain_ref,
    read_gain_ref,
    magnitude_ref,
    offset_ref,
    out_ref,
    new_hbm,
    in_ref,
    y_ref,
    w_ref,
    wo_ref,
    rates_ref,
    h_ref,
    x1_ref,
    xown_ref,
    mown_ref,
    sq_ref,
    sur_ref,
    state_ref,
    new_ref,
    proj_ref,
    rate_ref,
    grown_ref,
    qk_ref,
    xq_ref,
    kd_ref,
    u_ref,
    qs_ref,
    dec_ref,
    spread_ref,
    ones_ref,
    perm_ref,
    load_sem,
    state_sem,
    own_sem,
    in_sem,
    y_sem,
    sq_sem,
):
    f32, bf16 = jnp.float32, jnp.bfloat16
    me = lax.axis_index("tp")
    depth = count // 4
    core, row, line = lax.rem(me, 2), lax.rem(me // 2, 2), me // 4
    over, twin = me + 2 - 4 * row, me + 1 - 2 * core
    items = 2 * chunks
    rows = h_ref.shape[0]
    seqs, steps = qk_ref.shape[1], qk_ref.shape[2]
    width = in_ref.shape[3]
    heads = forget_hbm.shape[1]
    own_heads = heads // count

    loads = []
    for layer in range(2):
        for at, matrix in enumerate((probe_hbm, lookup_hbm, content_hbm, valve_hbm)):
            loads.append(
                (matrix.at[layer], w_ref.at[layer, :, pl.ds(at * LANES, LANES)])
            )
        loads.append((forget_hbm.at[layer], rates_ref.at[layer, pl.ds(0, heads), :]))
        loads.append((insert_hbm.at[layer], rates_ref.at[layer, pl.ds(heads, heads), :]))
        loads.append((emission_hbm.at[layer], wo_ref.at[layer]))
    loads = [
        pltpu.make_async_copy(source, target, load_sem.at[at])
        for at, (source, target) in enumerate(loads)
    ]
    for copy in loads:
        copy.start()

    def state_load(item):
        return pltpu.make_async_copy(
            states_hbm.at[item // chunks, pl.ds(lax.rem(item, chunks) * seqs, seqs)],
            state_ref.at[lax.rem(item, 2)],
            state_sem.at[0, lax.rem(item, 2)],
        )

    def state_store(item):
        return pltpu.make_async_copy(
            new_ref.at[lax.rem(item, 2)],
            new_hbm.at[item // chunks, pl.ds(lax.rem(item, chunks) * seqs, seqs)],
            state_sem.at[1, lax.rem(item, 2)],
        )

    state_load(0).start()

    barrier = pltpu.get_barrier_semaphore()
    for step in range(1, count):
        pl.semaphore_signal(
            barrier,
            inc=1,
            device_id={"tp": lax.rem(me + step, count)},
            device_id_type=pl.DeviceIdType.MESH,
        )
    pl.semaphore_wait(barrier, count - 1)

    def remote(source, target, send_sem, land_sem, device):
        return pltpu.make_async_remote_copy(
            src_ref=source,
            dst_ref=target,
            send_sem=send_sem,
            recv_sem=land_sem,
            device_id={"tp": device},
            device_id_type=pl.DeviceIdType.MESH,
        )

    def along(step):
        return 4 * (lax.rem(line + step, depth) - line)

    def begin(buf, sems, item, source):
        for step in range(1, depth):
            remote(
                source, buf.at[item, me], sems.at[0, item], sems.at[1, item], me + along(step)
            ).start()
        remote(source, buf.at[item, me], sems.at[0, item], sems.at[1, item], over).start()
        remote(source, buf.at[item, me], sems.at[0, item], sems.at[3, item], twin).start()

    def pass_on(buf, sems, item, origin, kind, device):
        block = buf.at[item, origin]
        remote(block, block, sems.at[0, item], sems.at[kind, item], device).start()

    def landed(buf, sems, item, kind, blocks):
        part = buf.at[item, pl.ds(0, blocks)]
        remote(part, part, sems.at[0, item], sems.at[kind, item], twin).wait_recv()

    def relay_over(buf, sems, item):
        landed(buf, sems, item, 1, depth)
        for step in range(1, depth):
            pass_on(buf, sems, item, me + along(depth - step), 2, over)
        for step in range(1, depth):
            pass_on(buf, sems, item, me + along(depth - step), 3, twin)
        pass_on(buf, sems, item, over, 3, twin)

    def relay_twin(buf, sems, item):
        landed(buf, sems, item, 2, depth - 1)
        for step in range(1, depth):
            pass_on(buf, sems, item, over + along(depth - step), 3, twin)

    def complete(buf, sems, item):
        landed(buf, sems, item, 3, 2 * depth)

    def drained(buf, sems, item):
        blocks = (depth + 1) + (2 * depth - 1) + (depth - 1)
        part = buf.at[item, pl.ds(0, blocks)]
        remote(part, part, sems.at[0, item], sems.at[1, item], twin).wait_send()

    def own_copy(item):
        return pltpu.make_async_copy(
            x_hbm.at[pl.ds(item * rows, rows), :], in_ref.at[item, me], own_sem.at[item]
        )

    def begin_x(item):
        begin(in_ref, in_sem, item, x_hbm.at[pl.ds(item * rows, rows), :])
        own_copy(item).start()

    begin_x(0)
    begin_x(1)

    def iota(shape, axis):
        return lax.broadcasted_iota(jnp.int32, shape, axis)

    shape = (2 * heads, 2 * LANES)
    wanted = iota(shape, 1) // HEAD_DIM
    wanted = jnp.where(wanted >= 2, wanted - 2 + heads, wanted) + me * own_heads
    spread_ref[...] = jnp.where(iota(shape, 0) == wanted, 1.0, 0.0).astype(bf16)
    shape = (2 * LANES, 2 * LANES)
    ones_ref[...] = jnp.where(
        iota(shape, 0) // HEAD_DIM == iota(shape, 1) // HEAD_DIM, 1.0, 0.0
    ).astype(bf16)
    shape = (LANES, LANES)
    head, channel = iota(shape, 0) // HEAD_DIM, iota(shape, 0) % HEAD_DIM
    target = (channel % 2) * HEAD_DIM + (channel // 2) * 2 + head
    perm_ref[...] = jnp.where(target == iota(shape, 1), 1.0, 0.0).astype(bf16)
    all_seqs = sur_ref.shape[1]
    first_head = iota((LANES, all_seqs), 0) < HEAD_DIM
    for layer in range(2):
        for step in range(steps):
            pair = surplus_ref[layer, step]
            wide = jnp.where(first_head, pair[0:1, :], pair[1:2, :])
            sur_ref[layer, :, step, :] = wide.T

    relay_over(in_ref, in_sem, 0)
    relay_twin(in_ref, in_sem, 0)
    for copy in loads:
        copy.wait()

    def squares(matrix):
        return matrix[:, :LANES] * matrix[:, :LANES] + matrix[:, LANES:] * matrix[:, LANES:]

    def inverse(total):
        return lax.rsqrt(jnp.sum(total, axis=1, keepdims=True) * (1.0 / D) + EPS)

    def cols_of(origin):
        return pl.ds(origin * width, width)

    def first_hidden(item):
        def part(group, carry):
            at = pl.ds(group * GROUP_ROWS, GROUP_ROWS)
            total = jnp.zeros((GROUP_ROWS, LANES), f32)
            for origin in range(count):
                total = total + squares(in_ref[item, origin, at, :].astype(f32))
            scale = inverse(total)
            for origin in range(count):
                block = in_ref[item, origin, at, :].astype(f32)
                gain = pre_gain_ref[0:1, cols_of(origin)]
                h_ref[at, cols_of(origin)] = (block * scale * gain).astype(bf16)
            return carry

        lax.fori_loop(0, rows // GROUP_ROWS, part, 0)

    def second_hidden(item):
        earlier = item - chunks

        def part(group, carry):
            at = pl.ds(group * GROUP_ROWS, GROUP_ROWS)
            total = jnp.zeros((GROUP_ROWS, LANES), f32)
            for origin in range(count):
                total = total + squares(in_ref[item, origin, at, :].astype(f32))
            scale = inverse(total)
            total = jnp.zeros((GROUP_ROWS, LANES), f32)
            for origin in range(count):
                mixed = in_ref[item, origin, at, :].astype(f32)
                before = in_ref[earlier, origin, at, :].astype(f32)
                gain = post_gain_ref[0:1, cols_of(origin)]
                after = (before + mixed * scale * gain).astype(bf16)
                x1_ref[origin, at, :] = after
                total = total + squares(after.astype(f32))
            scale = inverse(total)
            for origin in range(count):
                block = x1_ref[origin, at, :].astype(f32)
                gain = pre_gain_ref[1:2, cols_of(origin)]
                h_ref[at, cols_of(origin)] = (block * scale * gain).astype(bf16)
            xown_ref[earlier, at, :] = x1_ref[me, at, :]
            return carry

        lax.fori_loop(0, rows // GROUP_ROWS, part, 0)

    def cols(at):
        return proj_ref[:, at * LANES : (at + 1) * LANES].astype(f32)

    def tokens(matrix):
        return matrix.reshape(seqs, steps, LANES)

    def lane_pair(ref, layer):
        left = iota((1, LANES), 1) < HEAD_DIM
        return jnp.where(left, ref[layer, 0], ref[layer, 1])

    def prepare(layer, chunk):
        ones = ones_ref[...]
        perm = perm_ref[...]
        queries = jax.nn.silu(cols(0))
        keys = jax.nn.silu(cols(1))
        sums = head_sums(jnp.concatenate([queries * queries, keys * keys], axis=1), ones)
        queries = tokens(queries * lax.rsqrt(sums[:, :LANES] + EPS) * HEAD_DIM ** (-0.5))
        keys = tokens(keys * lax.rsqrt(sums[:, LANES:] + EPS))
        spread = bf16_dot(rate_ref[...], spread_ref[...])
        biased = spread[:, :LANES] + lane_pair(offset_ref, layer)
        softplus = jnp.maximum(biased, 0.0) + jnp.log1p(jnp.exp(-jnp.abs(biased)))
        pace = -jnp.exp(lane_pair(magnitude_ref, layer))
        cumulative = tokens(pace * softplus) + sur_ref[layer, pl.ds(chunk * seqs, seqs)]
        beta = tokens(jax.nn.sigmoid(spread[:, LANES:]))
        token = lax.broadcasted_iota(jnp.int32, (seqs, steps, LANES), 1)
        shift = 1
        while shift < steps:
            moved = pltpu.roll(cumulative, shift, axis=1)
            cumulative = cumulative + jnp.where(token >= shift, moved, 0.0)
            shift *= 2
        grown = jnp.exp(cumulative)
        grown_ref[...] = grown
        solved_u = beta * tokens(jax.nn.silu(cols(2)))
        solved_p = beta * grown * keys
        for at in range(steps):
            causal = token >= at
            gap = jnp.where(causal, cumulative - cumulative[:, at : at + 1, :], 0.0)
            decay = jnp.where(causal, jnp.exp(gap), 0.0)
            key_row = keys[:, at : at + 1, :]
            pair = jnp.concatenate([queries * key_row, keys * key_row], axis=2)
            dots = bf16_dot(pair.reshape(rows, 2 * LANES).astype(bf16), ones)
            qk_ref[at] = tokens(dots[:, :LANES]) * decay
            if at < steps - 1:
                a_col = jnp.where(token > at, beta * decay * tokens(dots[:, LANES:]), 0.0)
                solved_u = solved_u - a_col * solved_u[:, at : at + 1, :]
                solved_p = solved_p - a_col * solved_p[:, at : at + 1, :]
        last = cumulative[:, steps - 1 : steps, :]
        faded = keys * jnp.exp(last - cumulative)

        def permuted(first, second):
            both = jnp.concatenate([first, second], axis=1).reshape(2 * rows, LANES)
            return bf16_dot(both.astype(bf16), perm).astype(bf16).reshape(seqs, 2 * steps, LANES)

        xq_ref[...] = permuted(queries, solved_p)
        kd_ref[...] = permuted(faded, faded)
        u_ref[...] = solved_u
        dec_ref[...] = jnp.broadcast_to(jnp.exp(last), (seqs, steps, LANES))

    state_rows = state_ref.shape[2]

    def advance(slot):
        even = iota((state_rows, LANES), 0) % 2 == 0
        left = iota((state_rows, LANES), 1) < HEAD_DIM
        kept = even == left

        def one_sequence(at, carry):
            state = state_ref[slot, at]
            turned = pltpu.roll(state, HEAD_DIM, axis=1)
            upper = jnp.where(kept, jnp.where(even, state, turned), 0.0)
            lower = jnp.where(kept, jnp.where(even, turned, state), 0.0)
            wide = jnp.concatenate([upper, lower], axis=0).astype(bf16)
            read = bf16_dot(xq_ref[at], wide)
            qs_ref[at] = read[:steps]
            update = u_ref[at] - read[steps:]
            u_ref[at] = update
            high = update.astype(bf16).astype(f32)
            split = jnp.concatenate([high, update - high], axis=0).astype(bf16)
            grow = lax.dot_general(
                kd_ref[at], split, (((0,), (0,)), ((), ())), preferred_element_type=f32
            )
            grow_0, grow_1 = grow[:state_rows], grow[state_rows:]
            crossed = pltpu.roll(jnp.where(even, grow_1, grow_0), HEAD_DIM, axis=1)
            added = jnp.where(kept, jnp.where(even, grow_0, grow_1), crossed)
            fade = dec_ref[at]
            fade_turned = pltpu.roll(fade, HEAD_DIM, axis=1)
            copies = state_rows // steps
            factor = jnp.where(
                kept,
                jnp.concatenate([fade] * copies, axis=0),
                jnp.concatenate([fade_turned] * copies, axis=0),
            )
            new_ref[slot, at] = factor * state + added
            return carry

        lax.fori_loop(0, seqs, one_sequence, 0, unroll=8)

    def read_out(item, layer):
        update = u_ref[...]
        output = grown_ref[...] * qs_ref[...]
        for at in range(steps):
            output = output + qk_ref[at] * update[:, at : at + 1, :]
        output = output.reshape(rows, LANES)
        sums = head_sums(output * output, ones_ref[:LANES, :LANES])
        output = output * lax.rsqrt(sums * (1.0 / HEAD_DIM) + EPS)
        gain = read_gain_ref[pl.ds(layer, 1), :]
        y_ref[item, me] = (output * gain * jax.nn.silu(cols(3))).astype(bf16)

    def emit(item):
        whole = jnp.concatenate([y_ref[item, origin] for origin in range(count)], axis=1)
        return bf16_dot(whole, wo_ref[item // chunks]).astype(bf16)

    def emit_middle(item):
        in_ref[item + chunks, me] = emit(item)

    def emit_last(item):
        mixed = emit(item)
        chunk = item - chunks
        mown_ref[chunk] = mixed
        wide = mixed.astype(f32)
        total = jnp.sum(squares(wide), axis=1, keepdims=True)
        sq_ref[chunk, me] = jnp.broadcast_to(total, (rows, LANES)).T[:8]

    def sums_begin(chunk):
        block = sq_ref.at[chunk, me]
        for step in range(1, count):
            remote(
                block, block, sq_sem.at[0, chunk], sq_sem.at[1, chunk], lax.rem(me + step, count)
            ).start()

    def sums_all(chunk):
        part = sq_ref.at[chunk, pl.ds(0, count - 1)]
        return remote(part, part, sq_sem.at[0, chunk], sq_sem.at[1, chunk], twin)

    def finish(chunk):
        sums_all(chunk).wait_recv()
        total = sq_ref[chunk, 0]
        for origin in range(1, count):
            total = total + sq_ref[chunk, origin]
        total = jnp.broadcast_to(total[0:1, :], (LANES, rows)).T
        scale = lax.rsqrt(total * (1.0 / D) + EPS)
        for half in range(width // LANES):
            at = pl.ds(half * LANES, LANES)
            gain = post_gain_ref[1:2, pl.ds(pl.multiple_of(me * width + half * LANES, LANES), LANES)]
            before = xown_ref[chunk, :, at].astype(f32)
            mixed = mown_ref[chunk, :, at].astype(f32)
            out_ref[pl.ds(chunk * rows, rows), at] = (before + mixed * scale * gain).astype(bf16)

    lag = 3

    def slot_of(item, carry):
        layer, chunk, slot = item // chunks, lax.rem(item, chunks), lax.rem(item, 2)

        @pl.when(item + 1 < items)
        def _():
            state_load(item + 1).start()

        @pl.when(item + 2 < chunks)
        def _():
            begin_x(item + 2)

        complete(in_ref, in_sem, item)

        @pl.when(layer == 0)
        def _():
            own_copy(item).wait()
            first_hidden(item)

        @pl.when(layer == 1)
        def _():
            second_hidden(item)

        hidden = h_ref[...]
        proj_ref[...] = bf16_dot(hidden, w_ref[layer]).astype(bf16)
        rate_ref[...] = lax.dot_general(
            hidden, rates_ref[layer], (((1,), (1,)), ((), ())), preferred_element_type=f32
        ).astype(bf16)

        @pl.when(item >= 1)
        def _():
            relay_over(y_ref, y_sem, item - 1)

        prepare(layer, chunk)

        @pl.when(item + 1 < chunks)
        def _():
            relay_over(in_ref, in_sem, item + 1)

        @pl.when((item >= lag) & (item < lag + chunks))
        def _():
            relay_over(in_ref, in_sem, item + chunks - lag)

        state_load(item).wait()

        @pl.when(item >= 2)
        def _():
            state_store(item - 2).wait()

        advance(slot)

        @pl.when(item >= 1)
        def _():
            relay_twin(y_ref, y_sem, item - 1)

        read_out(item, layer)
        state_store(item).start()

        @pl.when(item >= 1)
        def _():
            complete(y_ref, y_sem, item - 1)

        begin(y_ref, y_sem, item, y_ref.at[item, me])

        @pl.when((item >= 1) & (item <= chunks))
        def _():
            emit_middle(item - 1)

        @pl.when(item > chunks)
        def _():
            emit_last(item - 1)

        @pl.when(item + 1 < chunks)
        def _():
            relay_twin(in_ref, in_sem, item + 1)

        @pl.when((item >= lag) & (item < lag + chunks))
        def _():
            relay_twin(in_ref, in_sem, item + chunks - lag)

        @pl.when((item >= 1) & (item <= chunks))
        def _():
            begin(in_ref, in_sem, item + chunks - 1, in_ref.at[item + chunks - 1, me])

        @pl.when(item > chunks)
        def _():
            sums_begin(item - 1 - chunks)

        return carry

    lax.fori_loop(0, items, slot_of, 0)
    final = items - 1
    relay_over(y_ref, y_sem, final)
    for chunk in range(chunks - 1):
        finish(chunk)
    relay_twin(y_ref, y_sem, final)
    state_store(final - 1).wait()
    state_store(final).wait()
    complete(y_ref, y_sem, final)
    emit_last(final)
    for item in range(items):
        drained(in_ref, in_sem, item)
        drained(y_ref, y_sem, item)
    sums_begin(chunks - 1)
    finish(chunks - 1)
    for chunk in range(chunks):
        sums_all(chunk).wait_send()


def local_two_heads(
    residual_channel,
    prior_block_multiplier,
    probe_map_matrix,
    lookup_map_matrix,
    content_map_matrix,
    emission_valve_matrix,
    forgetting_map_matrix,
    insertion_rate_matrix,
    forgetting_magnitude_exponent,
    channel_forgetting_offset,
    surplus_forgetting_amounts,
    readout_rescale_multiplier,
    emission_map_matrix,
    post_mixing_multiplier,
    recurrent_matrices,
):
    batch_total, steps, own_width = residual_channel.shape
    layers, _, head_count, state_size = recurrent_matrices.shape
    row_count = batch_total * steps
    count = lax.axis_size("tp")
    groups = state_size // LANES
    chunks = CHUNKS
    seqs, rows = batch_total // chunks, row_count // chunks
    heads = forgetting_map_matrix.shape[2]
    features = forgetting_map_matrix.shape[1]
    mix_width = emission_map_matrix.shape[1]
    states = (
        recurrent_matrices.reshape(layers, batch_total, head_count, groups, LANES)
        .transpose(0, 1, 3, 2, 4)
        .reshape(layers, batch_total, groups * head_count, LANES)
    )
    f32, bf16 = jnp.float32, jnp.bfloat16
    dma = pltpu.SemaphoreType.DMA
    hbm = pl.BlockSpec(memory_space=pl.ANY)
    vmem = pl.BlockSpec(memory_space=pltpu.VMEM)
    smem = pl.BlockSpec(memory_space=pltpu.SMEM)
    tile = (seqs, steps, LANES)
    state_tile = (2, seqs, groups * head_count, LANES)
    current, new_memory = pl.pallas_call(
        lambda *refs: step_kernel(count, chunks, *refs),
        out_shape=[
            jax.ShapeDtypeStruct((row_count, own_width), bf16),
            jax.ShapeDtypeStruct(states.shape, f32),
        ],
        in_specs=[hbm] * 9 + [vmem] * 4 + [smem] * 2,
        out_specs=[vmem, hbm],
        scratch_shapes=[
            pltpu.VMEM((2 * chunks, count, rows, own_width), bf16),
            pltpu.VMEM((2 * chunks, count, rows, LANES), bf16),
            pltpu.VMEM((layers, features, 4 * LANES), bf16),
            pltpu.VMEM((layers, mix_width, own_width), bf16),
            pltpu.VMEM((layers, 2 * heads, features), bf16),
            pltpu.VMEM((rows, features), bf16),
            pltpu.VMEM((count, rows, own_width), bf16),
            pltpu.VMEM((chunks, rows, own_width), bf16),
            pltpu.VMEM((chunks, rows, own_width), bf16),
            pltpu.VMEM((chunks, count, 8, rows), f32),
            pltpu.VMEM((layers, batch_total, steps, LANES), f32),
            pltpu.VMEM(state_tile, f32),
            pltpu.VMEM(state_tile, f32),
            pltpu.VMEM((rows, 4 * LANES), bf16),
            pltpu.VMEM((rows, 2 * heads), bf16),
            pltpu.VMEM(tile, f32),
            pltpu.VMEM((steps,) + tile, f32),
            pltpu.VMEM((seqs, 2 * steps, LANES), bf16),
            pltpu.VMEM((seqs, 2 * steps, LANES), bf16),
            pltpu.VMEM(tile, f32),
            pltpu.VMEM(tile, f32),
            pltpu.VMEM(tile, f32),
            pltpu.VMEM((2 * heads, 2 * LANES), bf16),
            pltpu.VMEM((2 * LANES, 2 * LANES), bf16),
            pltpu.VMEM((LANES, LANES), bf16),
            dma((14,)),
            dma((2, 2)),
            dma((chunks,)),
            dma((4, 2 * chunks)),
            dma((4, 2 * chunks)),
            dma((2, chunks)),
        ],
        compiler_params=pltpu.CompilerParams(
            collective_id=1, has_side_effects=True, vmem_limit_bytes=62 * 1024 * 1024
        ),
        name="step",
    )(
        residual_channel.reshape(row_count, own_width),
        probe_map_matrix,
        lookup_map_matrix,
        content_map_matrix,
        emission_valve_matrix,
        forgetting_map_matrix.transpose(0, 2, 1),
        insertion_rate_matrix.transpose(0, 2, 1),
        emission_map_matrix,
        states,
        surplus_forgetting_amounts.transpose(0, 2, 3, 1),
        prior_block_multiplier,
        post_mixing_multiplier,
        readout_rescale_multiplier,
        forgetting_magnitude_exponent,
        channel_forgetting_offset,
    )
    new_memory = (
        new_memory.reshape(layers, batch_total, groups, head_count, LANES)
        .transpose(0, 1, 3, 2, 4)
        .reshape(recurrent_matrices.shape)
    )
    return current.reshape(batch_total, steps, own_width), new_memory


def local_any(*arrays):
    residual_channel, recurrent_matrices = arrays[0], arrays[-1]
    two_heads = (
        recurrent_matrices.shape[2] * HEAD_DIM == LANES
        and residual_channel.shape[1] == 8
        and residual_channel.shape[0] % (8 * CHUNKS) == 0
        and residual_channel.shape[2] % LANES == 0
        and lax.axis_size("tp") % 4 == 0
        and lax.axis_size("tp") > 4
    )
    return (local_two_heads if two_heads else local)(*arrays)


def solution(mesh):
    return jax.shard_map(
        local_any,
        mesh=mesh,
        in_specs=(
            P("grp", None, "tp"),
            P(),
            P(None, None, "tp"),
            P(None, None, "tp"),
            P(None, None, "tp"),
            P(None, None, "tp"),
            P(),
            P(),
            P(None, "tp"),
            P(None, "tp"),
            P(None, "grp", None, "tp"),
            P(None, "tp"),
            P(None, None, "tp"),
            P(),
            P(None, "grp", "tp", None),
        ),
        out_specs=(P("grp", None, "tp"), P(None, "grp", "tp", None)),
        check_vma=False,
    )
```

time: 329 us -> 218 us (0.66)
  waiting for transfers between devices: 43.7 us -> 0 us
  local copies, waits for them, and re-layouts: 37.8 us -> 9.24 us
  Pallas kernels: 180 us -> 208 us
  matrix products: 26 us -> 0 us
  other arithmetic: 25.6 us -> 0 us
  between operations: 14.3 us -> 0.64 us
    all_gather x1 -> x0, waiting for transfers between devices: 43 us -> none  [local_two_heads(): lax.all_gather(residual_channel.reshape(row_count, own_width), 'tp', axis...]
    pallas_call x6 -> x1, Pallas kernels: 180 us -> 208 us  [local_two_heads(): pl.pallas_call(lambda *refs: step_kernel(count, chunks, *refs), out_shape...]
    dot_general x4 -> x0, matrix products: 26 us -> none  [the longest x2 18.3 us: local_two_heads(): jnp.dot(hidden, weights[layer], preferred_element_type=jnp.float32)]
    concatenate x2 -> x0, local copies, waits for them, and re-layouts: 20.1 us -> none  [local_two_heads(): jnp.concatenate([matrix[layer] for matrix in (probe_map_matrix, lookup_ma...]
    reduce_sum x4 -> x0, other arithmetic: 12.9 us -> none  [the longest x2 6.91 us: local_two_heads(): jnp.mean(widened * widened, axis=-1, keepdims=True) + EPS]
    squeeze x8 -> x0, local copies, waits for them, and re-layouts: 12 us -> none  [the longest x7 11.4 us: local_two_heads(): matrix[layer]]
    convert_element_type x4 -> x0, other arithmetic: 9.13 us -> none  [the longest x1 6.95 us: post_residual(): (widened + mixed_wide * post_rms * multiplier_terms_array).astype(jnp.bfl...]
    unnamed x24 -> x2, local copies, waits for them, and re-layouts: 1.16 us -> 9.24 us
  transfers between devices with their start and end apart: 1 -> 0, of which waited for: 1 -> 0; matrix products, arithmetic and copies ran while one was open for 12% -> 0% of each run, Pallas kernels for 0% -> 0%
where the time goes in v1:
time: 218 us
  Pallas kernels  208 us (95%)
  local copies, waits for them, and re-layouts  9.24 us (4%)
    pallas_call x1, Pallas kernels, local_two_heads(): pl.pallas_call(lambda *refs: step_kernel(count, chunks, *refs), out_shape...  208 us
    unnamed x2, local copies, waits for them, and re-layouts  9.24 us

profile of v1, /device:TPU:0, one launch (start us, length us, event | category | flops | bytes accessed | tf_op | source)
XLA Modules:
  0.0 218.2 jit_solution(15958617352625392659)
XLA Ops:
  0.6 208.3 %step.1 = (bf16[1024,256]{1,0:T(8,128)(2,1)}, f32[2,128,64,128]{3,2,1,0:T(8,128)}) custom-call(bf16[1024,256]{1,0:T(8,128)(2,1)} %bitcast.17, bf16[2,4096,128]{2,1,0:T(8,128)(2,1)} %refs_1_.1, bf16[2,4096,128]{2,1,0:T(8,128)(2,1)} %refs_2_.1, bf16[2,4096,128]{2,1,0:T(8,128)(2,1)} %refs_3_.1, bf16[2,4096,128]{2,1,0:T(8,128)(2,1)} %refs_4_.1, ...), custom_call_target="tpu_custom_call" | custom-call | tf_op jit(solution)/shard_map/step/pallas_call | solution.py:792
  208.9 1.9 copy.21
  210.8 7.4 %copy.22 = f32[2,128,2,4096]{3,2,1,0:T(2,128)} copy(f32[2,128,2,4096]{3,2,1,0:T(2,128)} %bitcast.16) | data formatting | bytes 16777216

commit v2 on v1

--- a/solution.py
+++ b/solution.py
@@ -242,7 +242,7 @@
     )
 
 
-CHUNKS = 4
+CHUNKS = 8
 GROUP_ROWS = 64
 
 
@@ -258,12 +258,12 @@
     insert_hbm,
     emission_hbm,
     states_hbm,
-    surplus_ref,
-    pre_gain_ref,
-    post_gain_ref,
-    read_gain_ref,
-    magnitude_ref,
-    offset_ref,
+    surplus_hbm,
+    pre_gain_hbm,
+    post_gain_hbm,
+    read_gain_hbm,
+    magnitude_hbm,
+    offset_hbm,
     out_ref,
     new_hbm,
     in_ref,
@@ -280,7 +280,6 @@
     state_ref,
     new_ref,
     proj_ref,
-    rate_ref,
     grown_ref,
     qk_ref,
     xq_ref,
@@ -291,6 +290,12 @@
     spread_ref,
     ones_ref,
     perm_ref,
+    surplus_ref,
+    pre_gain_ref,
+    post_gain_ref,
+    read_gain_ref,
+    magnitude_ref,
+    offset_ref,
     load_sem,
     state_sem,
     own_sem,
@@ -310,6 +315,15 @@
     heads = forget_hbm.shape[1]
     own_heads = heads // count
 
+    barrier = pltpu.get_barrier_semaphore()
+    for step in range(1, count):
+        pl.semaphore_signal(
+            barrier,
+            inc=1,
+            device_id={"tp": lax.rem(me + step, count)},
+            device_id_type=pl.DeviceIdType.MESH,
+        )
+
     loads = []
     for layer in range(2):
         for at, matrix in enumerate((probe_hbm, lookup_hbm, content_hbm, valve_hbm)):
@@ -319,6 +333,14 @@
         loads.append((forget_hbm.at[layer], rates_ref.at[layer, pl.ds(0, heads), :]))
         loads.append((insert_hbm.at[layer], rates_ref.at[layer, pl.ds(heads, heads), :]))
         loads.append((emission_hbm.at[layer], wo_ref.at[layer]))
+    loads += [
+        (surplus_hbm, surplus_ref),
+        (pre_gain_hbm, pre_gain_ref),
+        (post_gain_hbm, post_gain_ref),
+        (read_gain_hbm, read_gain_ref),
+        (magnitude_hbm, magnitude_ref),
+        (offset_hbm, offset_ref),
+    ]
     loads = [
         pltpu.make_async_copy(source, target, load_sem.at[at])
         for at, (source, target) in enumerate(loads)
@@ -342,14 +364,6 @@
 
     state_load(0).start()
 
-    barrier = pltpu.get_barrier_semaphore()
-    for step in range(1, count):
-        pl.semaphore_signal(
-            barrier,
-            inc=1,
-            device_id={"tp": lax.rem(me + step, count)},
-            device_id_type=pl.DeviceIdType.MESH,
-        )
     pl.semaphore_wait(barrier, count - 1)
 
     def remote(source, target, send_sem, land_sem, device):
@@ -411,8 +425,8 @@
         begin(in_ref, in_sem, item, x_hbm.at[pl.ds(item * rows, rows), :])
         own_copy(item).start()
 
-    begin_x(0)
-    begin_x(1)
+    for item in range(3):
+        begin_x(item)
 
     def iota(shape, axis):
         return lax.broadcasted_iota(jnp.int32, shape, axis)
@@ -429,6 +443,8 @@
     head, channel = iota(shape, 0) // HEAD_DIM, iota(shape, 0) % HEAD_DIM
     target = (channel % 2) * HEAD_DIM + (channel // 2) * 2 + head
     perm_ref[...] = jnp.where(target == iota(shape, 1), 1.0, 0.0).astype(bf16)
+    for copy in loads:
+        copy.wait()
     all_seqs = sur_ref.shape[1]
     first_head = iota((LANES, all_seqs), 0) < HEAD_DIM
     for layer in range(2):
@@ -436,11 +452,15 @@
             pair = surplus_ref[layer, step]
             wide = jnp.where(first_head, pair[0:1, :], pair[1:2, :])
             sur_ref[layer, :, step, :] = wide.T
+        for origin in range(count):
+            at = pl.ds(origin * width, width)
+            pair = rates_ref[layer, :, at].astype(f32)
+            filled = jnp.concatenate([pair, jnp.zeros((LANES - 2 * heads, width), f32)], axis=0)
+            w_ref[layer, at, pl.ds(4 * LANES, LANES)] = filled.T.astype(bf16)
 
     relay_over(in_ref, in_sem, 0)
     relay_twin(in_ref, in_sem, 0)
-    for copy in loads:
-        copy.wait()
+    relay_over(in_ref, in_sem, 1)
 
     def squares(matrix):
         return matrix[:, :LANES] * matrix[:, :LANES] + matrix[:, LANES:] * matrix[:, LANES:]
@@ -511,7 +531,7 @@
         sums = head_sums(jnp.concatenate([queries * queries, keys * keys], axis=1), ones)
         queries = tokens(queries * lax.rsqrt(sums[:, :LANES] + EPS) * HEAD_DIM ** (-0.5))
         keys = tokens(keys * lax.rsqrt(sums[:, LANES:] + EPS))
-        spread = bf16_dot(rate_ref[...], spread_ref[...])
+        spread = bf16_dot(proj_ref[:, 4 * LANES : 4 * LANES + 2 * heads], spread_ref[...])
         biased = spread[:, :LANES] + lane_pair(offset_ref, layer)
         softplus = jnp.maximum(biased, 0.0) + jnp.log1p(jnp.exp(-jnp.abs(biased)))
         pace = -jnp.exp(lane_pair(magnitude_ref, layer))
@@ -613,7 +633,7 @@
         mown_ref[chunk] = mixed
         wide = mixed.astype(f32)
         total = jnp.sum(squares(wide), axis=1, keepdims=True)
-        sq_ref[chunk, me] = jnp.broadcast_to(total, (rows, LANES)).T[:8]
+        sq_ref[chunk, me] = jnp.broadcast_to(total, (rows, LANES)).T[:1]
 
     def sums_begin(chunk):
         block = sq_ref.at[chunk, me]
@@ -631,7 +651,7 @@
         total = sq_ref[chunk, 0]
         for origin in range(1, count):
             total = total + sq_ref[chunk, origin]
-        total = jnp.broadcast_to(total[0:1, :], (LANES, rows)).T
+        total = jnp.broadcast_to(total, (LANES, rows)).T
         scale = lax.rsqrt(total * (1.0 / D) + EPS)
         for half in range(width // LANES):
             at = pl.ds(half * LANES, LANES)
@@ -640,19 +660,15 @@
             mixed = mown_ref[chunk, :, at].astype(f32)
             out_ref[pl.ds(chunk * rows, rows), at] = (before + mixed * scale * gain).astype(bf16)
 
-    lag = 3
+    def when(condition, action, *operands):
+        @pl.when(condition)
+        def _():
+            action(*operands)
 
     def slot_of(item, carry):
         layer, chunk, slot = item // chunks, lax.rem(item, chunks), lax.rem(item, 2)
-
-        @pl.when(item + 1 < items)
-        def _():
-            state_load(item + 1).start()
-
-        @pl.when(item + 2 < chunks)
-        def _():
-            begin_x(item + 2)
-
+        when(item + 1 < items, lambda: state_load(item + 1).start())
+        when(item + 3 < chunks, lambda: begin_x(item + 3))
         complete(in_ref, in_sem, item)
 
         @pl.when(layer == 0)
@@ -660,91 +676,57 @@
             own_copy(item).wait()
             first_hidden(item)
 
-        @pl.when(layer == 1)
-        def _():
-            second_hidden(item)
-
-        hidden = h_ref[...]
-        proj_ref[...] = bf16_dot(hidden, w_ref[layer]).astype(bf16)
-        rate_ref[...] = lax.dot_general(
-            hidden, rates_ref[layer], (((1,), (1,)), ((), ())), preferred_element_type=f32
-        ).astype(bf16)
-
-        @pl.when(item >= 1)
-        def _():
-            relay_over(y_ref, y_sem, item - 1)
-
+        when(layer == 1, second_hidden, item)
+        proj_ref[...] = bf16_dot(h_ref[...], w_ref[layer]).astype(bf16)
+
+        when(item >= 2, relay_twin, y_ref, y_sem, item - 2)
+        when((item >= 4) & (item < 4 + chunks), relay_over, in_ref, in_sem, item - 4 + chunks)
+        when((item >= 5) & (item < 5 + chunks), relay_twin, in_ref, in_sem, item - 5 + chunks)
+        when(item + 1 < chunks, relay_twin, in_ref, in_sem, item + 1)
         prepare(layer, chunk)
-
-        @pl.when(item + 1 < chunks)
-        def _():
-            relay_over(in_ref, in_sem, item + 1)
-
-        @pl.when((item >= lag) & (item < lag + chunks))
-        def _():
-            relay_over(in_ref, in_sem, item + chunks - lag)
-
         state_load(item).wait()
-
-        @pl.when(item >= 2)
-        def _():
-            state_store(item - 2).wait()
-
+        when(item >= 2, lambda: state_store(item - 2).wait())
         advance(slot)
-
-        @pl.when(item >= 1)
-        def _():
-            relay_twin(y_ref, y_sem, item - 1)
-
+        when(item >= 1, relay_over, y_ref, y_sem, item - 1)
+        when(item + 2 < chunks, relay_over, in_ref, in_sem, item + 2)
         read_out(item, layer)
         state_store(item).start()
-
-        @pl.when(item >= 1)
+        when(item >= 2, complete, y_ref, y_sem, item - 2)
+        begin(y_ref, y_sem, item, y_ref.at[item, me])
+        early = (item >= 2) & (item < chunks + 2)
+        when(early, emit_middle, item - 2)
+        when(item >= chunks + 2, emit_last, item - 2)
+
+        @pl.when(early)
         def _():
-            complete(y_ref, y_sem, item - 1)
-
-        begin(y_ref, y_sem, item, y_ref.at[item, me])
-
-        @pl.when((item >= 1) & (item <= chunks))
-        def _():
-            emit_middle(item - 1)
-
-        @pl.when(item > chunks)
-        def _():
-            emit_last(item - 1)
-
-        @pl.when(item + 1 < chunks)
-        def _():
-            relay_twin(in_ref, in_sem, item + 1)
-
-        @pl.when((item >= lag) & (item < lag + chunks))
-        def _():
-            relay_twin(in_ref, in_sem, item + chunks - lag)
-
-        @pl.when((item >= 1) & (item <= chunks))
-        def _():
-            begin(in_ref, in_sem, item + chunks - 1, in_ref.at[item + chunks - 1, me])
-
-        @pl.when(item > chunks)
-        def _():
-            sums_begin(item - 1 - chunks)
-
+            made = item - 2 + chunks
+            begin(in_ref, in_sem, made, in_ref.at[made, me])
+
+        when(item >= chunks + 2, sums_begin, item - 2 - chunks)
         return carry
 
     lax.fori_loop(0, items, slot_of, 0)
     final = items - 1
+    relay_twin(y_ref, y_sem, final - 1)
+    for chunk in range(chunks - 3):
+        finish(chunk)
     relay_over(y_ref, y_sem, final)
-    for chunk in range(chunks - 1):
-        finish(chunk)
+    complete(y_ref, y_sem, final - 1)
+    emit_last(final - 1)
+    finish(chunks - 3)
     relay_twin(y_ref, y_sem, final)
+    sums_begin(chunks - 2)
     state_store(final - 1).wait()
     state_store(final).wait()
+    for item in range(items):
+        drained(in_ref, in_sem, item)
+        if item < final:
+            drained(y_ref, y_sem, item)
     complete(y_ref, y_sem, final)
     emit_last(final)
-    for item in range(items):
-        drained(in_ref, in_sem, item)
-        drained(y_ref, y_sem, item)
+    drained(y_ref, y_sem, final)
     sums_begin(chunks - 1)
+    finish(chunks - 2)
     finish(chunks - 1)
     for chunk in range(chunks):
         sums_all(chunk).wait_send()
@@ -786,7 +768,6 @@
     dma = pltpu.SemaphoreType.DMA
     hbm = pl.BlockSpec(memory_space=pl.ANY)
     vmem = pl.BlockSpec(memory_space=pltpu.VMEM)
-    smem = pl.BlockSpec(memory_space=pltpu.SMEM)
     tile = (seqs, steps, LANES)
     state_tile = (2, seqs, groups * head_count, LANES)
     current, new_memory = pl.pallas_call(
@@ -795,24 +776,23 @@
             jax.ShapeDtypeStruct((row_count, own_width), bf16),
             jax.ShapeDtypeStruct(states.shape, f32),
         ],
-        in_specs=[hbm] * 9 + [vmem] * 4 + [smem] * 2,
+        in_specs=[hbm] * 15,
         out_specs=[vmem, hbm],
         scratch_shapes=[
             pltpu.VMEM((2 * chunks, count, rows, own_width), bf16),
             pltpu.VMEM((2 * chunks, count, rows, LANES), bf16),
-            pltpu.VMEM((layers, features, 4 * LANES), bf16),
+            pltpu.VMEM((layers, features, 5 * LANES), bf16),
             pltpu.VMEM((layers, mix_width, own_width), bf16),
             pltpu.VMEM((layers, 2 * heads, features), bf16),
             pltpu.VMEM((rows, features), bf16),
             pltpu.VMEM((count, rows, own_width), bf16),
             pltpu.VMEM((chunks, rows, own_width), bf16),
             pltpu.VMEM((chunks, rows, own_width), bf16),
-            pltpu.VMEM((chunks, count, 8, rows), f32),
+            pltpu.VMEM((chunks, count, 1, rows), f32),
             pltpu.VMEM((layers, batch_total, steps, LANES), f32),
             pltpu.VMEM(state_tile, f32),
             pltpu.VMEM(state_tile, f32),
-            pltpu.VMEM((rows, 4 * LANES), bf16),
-            pltpu.VMEM((rows, 2 * heads), bf16),
+            pltpu.VMEM((rows, 5 * LANES), bf16),
             pltpu.VMEM(tile, f32),
             pltpu.VMEM((steps,) + tile, f32),
             pltpu.VMEM((seqs, 2 * steps, LANES), bf16),
@@ -823,7 +803,13 @@
             pltpu.VMEM((2 * heads, 2 * LANES), bf16),
             pltpu.VMEM((2 * LANES, 2 * LANES), bf16),
             pltpu.VMEM((LANES, LANES), bf16),
-            dma((14,)),
+            pltpu.VMEM((layers, steps, head_count, batch_total), f32),
+            pltpu.VMEM((layers, features), f32),
+            pltpu.VMEM((layers, features), f32),
+            pltpu.VMEM((layers, LANES), f32),
+            pltpu.SMEM((layers, head_count), f32),
+            pltpu.SMEM((layers, head_count), f32),
+            dma((20,)),
             dma((2, 2)),
             dma((chunks,)),
             dma((4, 2 * chunks)),

time: 218 us -> 196 us (0.90)
  Pallas kernels: 208 us -> 186 us
    pallas_call x1, Pallas kernels: 208 us -> 186 us  [local_two_heads(): pl.pallas_call(lambda *refs: step_kernel(count, chunks, *refs), out_shape...]
where the time goes in v2:
time: 196 us
  Pallas kernels  186 us (95%)
  local copies, waits for them, and re-layouts  9.24 us (5%)
    pallas_call x1, Pallas kernels, local_two_heads(): pl.pallas_call(lambda *refs: step_kernel(count, chunks, *refs), out_shape...  186 us
    unnamed x2, local copies, waits for them, and re-layouts  9.24 us

profile of v2, /device:TPU:0, one launch (start us, length us, event | category | flops | bytes accessed | tf_op | source)
XLA Modules:
  0.0 195.9 jit_solution(3900236552522572784)
XLA Ops:
  0.6 186.0 %step.1 = (bf16[1024,256]{1,0:T(8,128)(2,1)}, f32[2,128,64,128]{3,2,1,0:T(8,128)}) custom-call(bf16[1024,256]{1,0:T(8,128)(2,1)} %bitcast.17, bf16[2,4096,128]{2,1,0:T(8,128)(2,1)} %refs_1_.1, bf16[2,4096,128]{2,1,0:T(8,128)(2,1)} %refs_2_.1, bf16[2,4096,128]{2,1,0:T(8,128)(2,1)} %refs_3_.1, bf16[2,4096,128]{2,1,0:T(8,128)(2,1)} %refs_4_.1, ...), custom_call_target="tpu_custom_call" | custom-call | tf_op jit(solution)/shard_map/step/pallas_call | solution.py:773
  186.6 1.9 copy.21
  188.5 7.4 %copy.22 = f32[2,128,2,4096]{3,2,1,0:T(2,128)} copy(f32[2,128,2,4096]{3,2,1,0:T(2,128)} %bitcast.16) | data formatting | bytes 16777216

commit v3 on v2

--- a/solution.py
+++ b/solution.py
@@ -243,6 +243,7 @@
 
 
 CHUNKS = 8
+AHEAD = 8
 GROUP_ROWS = 64
 
 
@@ -348,18 +349,31 @@
     for copy in loads:
         copy.start()
 
-    def state_load(item):
+    def place(slot):
+        past = slot - AHEAD
+        odd = lax.rem(past + 2 * AHEAD, 2)
+        layer = jnp.where(slot < AHEAD, 0, jnp.where(slot < items - AHEAD, 1 - odd, 1))
+        middle = jnp.where(slot < items - AHEAD, past // 2 + AHEAD * odd, slot - chunks)
+        return layer, jnp.where(slot < AHEAD, slot, middle)
+
+    def item_at(slot):
+        layer, chunk = place(slot)
+        return layer * chunks + chunk
+
+    def state_load(slot):
+        layer, chunk = place(slot)
         return pltpu.make_async_copy(
-            states_hbm.at[item // chunks, pl.ds(lax.rem(item, chunks) * seqs, seqs)],
-            state_ref.at[lax.rem(item, 2)],
-            state_sem.at[0, lax.rem(item, 2)],
+            states_hbm.at[layer, pl.ds(chunk * seqs, seqs)],
+            state_ref.at[lax.rem(slot, 2)],
+            state_sem.at[0, lax.rem(slot, 2)],
         )
 
-    def state_store(item):
+    def state_store(slot):
+        layer, chunk = place(slot)
         return pltpu.make_async_copy(
-            new_ref.at[lax.rem(item, 2)],
-            new_hbm.at[item // chunks, pl.ds(lax.rem(item, chunks) * seqs, seqs)],
-            state_sem.at[1, lax.rem(item, 2)],
+            new_ref.at[lax.rem(slot, 2)],
+            new_hbm.at[layer, pl.ds(chunk * seqs, seqs)],
+            state_sem.at[1, lax.rem(slot, 2)],
         )
 
     state_load(0).start()
@@ -376,45 +390,71 @@
             device_id_type=pl.DeviceIdType.MESH,
         )
 
+    def when(condition, action, *operands):
+        @pl.when(condition)
+        def _():
+            action(*operands)
+
+    inner = (line == 1) | (line == 2)
+    shifts = (0, 1 - 2 * lax.rem(line, 2), 2 - 4 * (line // 2), 3 - 2 * line)
+
     def along(step):
-        return 4 * (lax.rem(line + step, depth) - line)
+        return 4 * shifts[step]
 
     def begin(buf, sems, item, source):
-        for step in range(1, depth):
-            remote(
-                source, buf.at[item, me], sems.at[0, item], sems.at[1, item], me + along(step)
-            ).start()
-        remote(source, buf.at[item, me], sems.at[0, item], sems.at[1, item], over).start()
-        remote(source, buf.at[item, me], sems.at[0, item], sems.at[3, item], twin).start()
-
-    def pass_on(buf, sems, item, origin, kind, device):
+        target = buf.at[item, me]
+
+        def out(kind, device):
+            remote(source, target, sems.at[0, item], sems.at[kind, item], device).start()
+
+        out(5, me + along(2))
+        out(4, me + along(1))
+        when(inner, out, 6, me + along(3))
+        out(1, over)
+        out(3, twin)
+
+    def pass_on(buf, sems, item, origin, kind, device, half=None):
         block = buf.at[item, origin]
+        if half is not None:
+            block = buf.at[item, origin, pl.ds(half * (rows // 2), rows // 2)]
         remote(block, block, sems.at[0, item], sems.at[kind, item], device).start()
 
     def landed(buf, sems, item, kind, blocks):
         part = buf.at[item, pl.ds(0, blocks)]
         remote(part, part, sems.at[0, item], sems.at[kind, item], twin).wait_recv()
 
-    def relay_over(buf, sems, item):
-        landed(buf, sems, item, 1, depth)
-        for step in range(1, depth):
-            pass_on(buf, sems, item, me + along(depth - step), 2, over)
-        for step in range(1, depth):
-            pass_on(buf, sems, item, me + along(depth - step), 3, twin)
+    def relay_near(buf, sems, item):
+        landed(buf, sems, item, 5, 1)
+        when(inner, pass_on, buf, sems, item, me + along(2), 6, me + along(1))
+        pass_on(buf, sems, item, me + along(2), 2, over)
+        pass_on(buf, sems, item, me + along(2), 3, twin)
+        landed(buf, sems, item, 1, 1)
+        pass_on(buf, sems, item, over, 2, me + along(1), 0)
         pass_on(buf, sems, item, over, 3, twin)
+        landed(buf, sems, item, 4, 1)
+        pass_on(buf, sems, item, me + along(1), 2, over, 1)
+        pass_on(buf, sems, item, me + along(1), 3, twin)
+
+    def relay_far(buf, sems, item):
+        landed(buf, sems, item, 6, 1)
+        pass_on(buf, sems, item, me + along(3), 2, over)
+        pass_on(buf, sems, item, me + along(3), 3, twin)
 
     def relay_twin(buf, sems, item):
         landed(buf, sems, item, 2, depth - 1)
         for step in range(1, depth):
-            pass_on(buf, sems, item, over + along(depth - step), 3, twin)
+            pass_on(buf, sems, item, over + along(step), 3, twin)
 
     def complete(buf, sems, item):
         landed(buf, sems, item, 3, 2 * depth)
 
     def drained(buf, sems, item):
-        blocks = (depth + 1) + (2 * depth - 1) + (depth - 1)
-        part = buf.at[item, pl.ds(0, blocks)]
-        remote(part, part, sems.at[0, item], sems.at[1, item], twin).wait_send()
+        def sent(blocks):
+            part = buf.at[item, pl.ds(0, blocks)]
+            remote(part, part, sems.at[0, item], sems.at[1, item], twin).wait_send()
+
+        when(inner, sent, count)
+        when(jnp.logical_not(inner), sent, count - 2)
 
     def own_copy(item):
         return pltpu.make_async_copy(
@@ -458,9 +498,9 @@
             filled = jnp.concatenate([pair, jnp.zeros((LANES - 2 * heads, width), f32)], axis=0)
             w_ref[layer, at, pl.ds(4 * LANES, LANES)] = filled.T.astype(bf16)
 
-    relay_over(in_ref, in_sem, 0)
+    relay_near(in_ref, in_sem, 0)
+    relay_far(in_ref, in_sem, 0)
     relay_twin(in_ref, in_sem, 0)
-    relay_over(in_ref, in_sem, 1)
 
     def squares(matrix):
         return matrix[:, :LANES] * matrix[:, :LANES] + matrix[:, LANES:] * matrix[:, LANES:]
@@ -660,64 +700,78 @@
             mixed = mown_ref[chunk, :, at].astype(f32)
             out_ref[pl.ds(chunk * rows, rows), at] = (before + mixed * scale * gain).astype(bf16)
 
-    def when(condition, action, *operands):
-        @pl.when(condition)
+    def slot_of(slot, carry):
+        (layer, chunk), buffer = place(slot), lax.rem(slot, 2)
+        item = layer * chunks + chunk
+        first = layer == 0
+        when(slot + 1 < items, lambda: state_load(slot + 1).start())
+        when(first & (chunk + 3 < chunks), lambda: begin_x(chunk + 3))
+        complete(in_ref, in_sem, item)
+
+        @pl.when(first)
         def _():
-            action(*operands)
-
-    def slot_of(item, carry):
-        layer, chunk, slot = item // chunks, lax.rem(item, chunks), lax.rem(item, 2)
-        when(item + 1 < items, lambda: state_load(item + 1).start())
-        when(item + 3 < chunks, lambda: begin_x(item + 3))
-        complete(in_ref, in_sem, item)
-
-        @pl.when(layer == 0)
-        def _():
-            own_copy(item).wait()
-            first_hidden(item)
+            own_copy(chunk).wait()
+            first_hidden(chunk)
 
         when(layer == 1, second_hidden, item)
         proj_ref[...] = bf16_dot(h_ref[...], w_ref[layer]).astype(bf16)
 
-        when(item >= 2, relay_twin, y_ref, y_sem, item - 2)
-        when((item >= 4) & (item < 4 + chunks), relay_over, in_ref, in_sem, item - 4 + chunks)
-        when((item >= 5) & (item < 5 + chunks), relay_twin, in_ref, in_sem, item - 5 + chunks)
-        when(item + 1 < chunks, relay_twin, in_ref, in_sem, item + 1)
+        def older(by):
+            return item_at(slot - by)
+
+        def mixed(by):
+            return (slot >= by) & (place(slot - by)[0] == 0)
+
+        when(mixed(5), relay_near, in_ref, in_sem, older(5) + chunks)
+        when(slot == 0, relay_near, in_ref, in_sem, 1)
+        when(slot >= 2, relay_far, y_ref, y_sem, older(2))
+        when(mixed(6), relay_twin, in_ref, in_sem, older(6) + chunks)
         prepare(layer, chunk)
-        state_load(item).wait()
-        when(item >= 2, lambda: state_store(item - 2).wait())
-        advance(slot)
-        when(item >= 1, relay_over, y_ref, y_sem, item - 1)
-        when(item + 2 < chunks, relay_over, in_ref, in_sem, item + 2)
+        when(first & (chunk + 2 < chunks), relay_near, in_ref, in_sem, chunk + 2)
+        when(slot == 0, relay_far, in_ref, in_sem, 1)
+        state_load(slot).wait()
+        when(slot >= 2, lambda: state_store(slot - 2).wait())
+        advance(buffer)
+        when(mixed(5), relay_far, in_ref, in_sem, older(5) + chunks)
+        when(slot >= 1, relay_near, y_ref, y_sem, older(1))
+        when(first & (chunk + 2 < chunks), relay_far, in_ref, in_sem, chunk + 2)
+        when(slot >= 2, relay_twin, y_ref, y_sem, older(2))
         read_out(item, layer)
-        state_store(item).start()
-        when(item >= 2, complete, y_ref, y_sem, item - 2)
+        state_store(slot).start()
+        past, (past_layer, past_chunk) = older(3), place(slot - 3)
+        when(slot >= 3, complete, y_ref, y_sem, past)
         begin(y_ref, y_sem, item, y_ref.at[item, me])
-        early = (item >= 2) & (item < chunks + 2)
-        when(early, emit_middle, item - 2)
-        when(item >= chunks + 2, emit_last, item - 2)
+        early = (slot >= 3) & (past_layer == 0)
+        late = (slot >= 3) & (past_layer == 1)
+        when(early, emit_middle, past)
+        when(late, emit_last, past)
+        when(first & (chunk + 1 < chunks), relay_twin, in_ref, in_sem, chunk + 1)
 
         @pl.when(early)
         def _():
-            made = item - 2 + chunks
-            begin(in_ref, in_sem, made, in_ref.at[made, me])
-
-        when(item >= chunks + 2, sums_begin, item - 2 - chunks)
+            begin(in_ref, in_sem, past + chunks, in_ref.at[past + chunks, me])
+
+        when(late, sums_begin, past_chunk)
         return carry
 
     lax.fori_loop(0, items, slot_of, 0)
     final = items - 1
+    relay_far(y_ref, y_sem, final - 1)
+    complete(y_ref, y_sem, final - 2)
+    emit_last(final - 2)
+    relay_near(y_ref, y_sem, final)
     relay_twin(y_ref, y_sem, final - 1)
-    for chunk in range(chunks - 3):
+    sums_begin(chunks - 3)
+    for chunk in range(chunks - 4):
         finish(chunk)
-    relay_over(y_ref, y_sem, final)
+    relay_far(y_ref, y_sem, final)
     complete(y_ref, y_sem, final - 1)
     emit_last(final - 1)
-    finish(chunks - 3)
+    finish(chunks - 4)
+    sums_begin(chunks - 2)
     relay_twin(y_ref, y_sem, final)
-    sums_begin(chunks - 2)
-    state_store(final - 1).wait()
-    state_store(final).wait()
+    state_store(items - 2).wait()
+    state_store(items - 1).wait()
     for item in range(items):
         drained(in_ref, in_sem, item)
         if item < final:
@@ -726,8 +780,8 @@
     emit_last(final)
     drained(y_ref, y_sem, final)
     sums_begin(chunks - 1)
-    finish(chunks - 2)
-    finish(chunks - 1)
+    for chunk in range(chunks - 3, chunks):
+        finish(chunk)
     for chunk in range(chunks):
         sums_all(chunk).wait_send()
 
@@ -812,8 +866,8 @@
             dma((20,)),
             dma((2, 2)),
             dma((chunks,)),
-            dma((4, 2 * chunks)),
-            dma((4, 2 * chunks)),
+            dma((3 + count // 4, 2 * chunks)),
+            dma((3 + count // 4, 2 * chunks)),
             dma((2, chunks)),
         ],
         compiler_params=pltpu.CompilerParams(
@@ -852,8 +906,7 @@
         and residual_channel.shape[1] == 8
         and residual_channel.shape[0] % (8 * CHUNKS) == 0
         and residual_channel.shape[2] % LANES == 0
-        and lax.axis_size("tp") % 4 == 0
-        and lax.axis_size("tp") > 4
+        and lax.axis_size("tp") == 16
     )
     return (local_two_heads if two_heads else local)(*arrays)
 

time: 196 us -> 176 us (0.90)
  Pallas kernels: 186 us -> 165 us
    pallas_call x1, Pallas kernels: 186 us -> 165 us  [local_two_heads(): pl.pallas_call(lambda *refs: step_kernel(count, chunks, *refs), out_shape...]
where the time goes in v3:
time: 176 us; the launch traced here: 175 us
  Pallas kernels  165 us (94%)
  local copies, waits for them, and re-layouts  9.24 us (5%)
    pallas_call x1, Pallas kernels, local_two_heads(): pl.pallas_call(lambda *refs: step_kernel(count, chunks, *refs), out_shape...  165 us
    unnamed x2, local copies, waits for them, and re-layouts  9.24 us

profile of v3, /device:TPU:0, one launch (start us, length us, event | category | flops | bytes accessed | tf_op | source)
XLA Modules:
  0.0 175.3 jit_solution(5994342980491045475)
XLA Ops:
  0.6 165.4 %step.1 = (bf16[1024,256]{1,0:T(8,128)(2,1)}, f32[2,128,64,128]{3,2,1,0:T(8,128)}) custom-call(bf16[1024,256]{1,0:T(8,128)(2,1)} %bitcast.17, bf16[2,4096,128]{2,1,0:T(8,128)(2,1)} %refs_1_.1, bf16[2,4096,128]{2,1,0:T(8,128)(2,1)} %refs_2_.1, bf16[2,4096,128]{2,1,0:T(8,128)(2,1)} %refs_3_.1, bf16[2,4096,128]{2,1,0:T(8,128)(2,1)} %refs_4_.1, ...), custom_call_target="tpu_custom_call" | custom-call | tf_op jit(solution)/shard_map/step/pallas_call | solution.py:827
  166.1 1.9 %copy.21 = bf16[128,8,256]{2,1,0:T(8,128)(2,1)} copy(bf16[128,8,256]{2,1,0:T(8,128)(2,1)} %bitcast.20) | data formatting | bytes 1048576
  168.0 7.4 %copy.22 = f32[2,128,2,4096]{3,2,1,0:T(2,128)} copy(f32[2,128,2,4096]{3,2,1,0:T(2,128)} %bitcast.16) | data formatting | bytes 16777216

commit v4 on v3

--- a/solution.py
+++ b/solution.py
@@ -266,7 +266,7 @@
     magnitude_hbm,
     offset_hbm,
     out_ref,
-    new_hbm,
+    new_ref,
     in_ref,
     y_ref,
     w_ref,
@@ -279,7 +279,6 @@
     sq_ref,
     sur_ref,
     state_ref,
-    new_ref,
     proj_ref,
     grown_ref,
     qk_ref,
@@ -365,15 +364,7 @@
         return pltpu.make_async_copy(
             states_hbm.at[layer, pl.ds(chunk * seqs, seqs)],
             state_ref.at[lax.rem(slot, 2)],
-            state_sem.at[0, lax.rem(slot, 2)],
-        )
-
-    def state_store(slot):
-        layer, chunk = place(slot)
-        return pltpu.make_async_copy(
-            new_ref.at[lax.rem(slot, 2)],
-            new_hbm.at[layer, pl.ds(chunk * seqs, seqs)],
-            state_sem.at[1, lax.rem(slot, 2)],
+            state_sem.at[lax.rem(slot, 2)],
         )
 
     state_load(0).start()
@@ -479,10 +470,11 @@
     ones_ref[...] = jnp.where(
         iota(shape, 0) // HEAD_DIM == iota(shape, 1) // HEAD_DIM, 1.0, 0.0
     ).astype(bf16)
-    shape = (LANES, LANES)
-    head, channel = iota(shape, 0) // HEAD_DIM, iota(shape, 0) % HEAD_DIM
-    target = (channel % 2) * HEAD_DIM + (channel // 2) * 2 + head
-    perm_ref[...] = jnp.where(target == iota(shape, 1), 1.0, 0.0).astype(bf16)
+    shape = (LANES, 4 * LANES)
+    block, spot = iota(shape, 1) // LANES, iota(shape, 1) % LANES
+    target = (block // 2) * HEAD_DIM + 2 * (spot // 2) + block % 2
+    fits = (iota(shape, 0) == target) & (spot % 2 == block // 2) & (spot < HEAD_DIM)
+    perm_ref[...] = jnp.where(fits, 1.0, 0.0).astype(bf16)
     for copy in loads:
         copy.wait()
     all_seqs = sur_ref.shape[1]
@@ -602,49 +594,58 @@
         last = cumulative[:, steps - 1 : steps, :]
         faded = keys * jnp.exp(last - cumulative)
 
-        def permuted(first, second):
-            both = jnp.concatenate([first, second], axis=1).reshape(2 * rows, LANES)
-            return bf16_dot(both.astype(bf16), perm).astype(bf16).reshape(seqs, 2 * steps, LANES)
-
-        xq_ref[...] = permuted(queries, solved_p)
-        kd_ref[...] = permuted(faded, faded)
+        def scattered(matrix):
+            placed = bf16_dot(matrix.reshape(-1, LANES).astype(bf16), perm)
+            blocks = [placed[:, at * LANES : (at + 1) * LANES] for at in range(4)]
+            return [block.reshape(seqs, -1, LANES) for block in blocks]
+
+        for at, block in enumerate(scattered(jnp.concatenate([queries, solved_p], axis=1))):
+            xq_ref[:, at * 2 * steps : (at + 1) * 2 * steps, :] = block.astype(bf16)
+        blocks = scattered(faded)
+        for at in (0, 2):
+            both = jnp.concatenate([blocks[at], blocks[at + 1]], axis=1).astype(bf16)
+            kd_ref[:, at * steps : (at + 2) * steps, :] = both
+            kd_ref[:, (at + 4) * steps : (at + 6) * steps, :] = both
         u_ref[...] = solved_u
-        dec_ref[...] = jnp.broadcast_to(jnp.exp(last), (seqs, steps, LANES))
+        fade = jnp.broadcast_to(jnp.exp(last), (seqs, steps, LANES))
+        lane = lax.broadcasted_iota(jnp.int32, (seqs, steps, LANES), 2)
+        kept = (token % 2 == 0) == (lane < HEAD_DIM)
+        dec_ref[...] = jnp.where(kept, fade, pltpu.roll(fade, HEAD_DIM, axis=2))
 
     state_rows = state_ref.shape[2]
 
-    def advance(slot):
-        even = iota((state_rows, LANES), 0) % 2 == 0
-        left = iota((state_rows, LANES), 1) < HEAD_DIM
-        kept = even == left
+    def advance(slot, layer, chunk):
+        pair_left = iota((2 * steps, LANES), 1) < HEAD_DIM
+        left = iota((steps, LANES), 1) < HEAD_DIM
 
         def one_sequence(at, carry):
             state = state_ref[slot, at]
-            turned = pltpu.roll(state, HEAD_DIM, axis=1)
-            upper = jnp.where(kept, jnp.where(even, state, turned), 0.0)
-            lower = jnp.where(kept, jnp.where(even, turned, state), 0.0)
-            wide = jnp.concatenate([upper, lower], axis=0).astype(bf16)
-            read = bf16_dot(xq_ref[at], wide)
+            read = bf16_dot(xq_ref[at, :, pl.ds(0, state_rows)], state.astype(bf16))
+            parts = [read[2 * steps * b : 2 * steps * (b + 1)] for b in range(4)]
+            straight = jnp.where(pair_left, parts[0], parts[3])
+            crossed = jnp.where(pair_left, parts[2], parts[1])
+            read = straight + pltpu.roll(crossed, HEAD_DIM, axis=1)
             qs_ref[at] = read[:steps]
             update = u_ref[at] - read[steps:]
             u_ref[at] = update
             high = update.astype(bf16).astype(f32)
-            split = jnp.concatenate([high, update - high], axis=0).astype(bf16)
+            spread = []
+            for part in (high, update - high):
+                turned = pltpu.roll(part, HEAD_DIM, axis=1)
+                spread += [
+                    jnp.where(left, part, 0.0),
+                    jnp.where(left, 0.0, turned),
+                    jnp.where(left, turned, 0.0),
+                    jnp.where(left, 0.0, part),
+                ]
             grow = lax.dot_general(
-                kd_ref[at], split, (((0,), (0,)), ((), ())), preferred_element_type=f32
+                kd_ref[at, :, pl.ds(0, state_rows)],
+                jnp.concatenate(spread, axis=0).astype(bf16),
+                (((0,), (0,)), ((), ())),
+                preferred_element_type=f32,
             )
-            grow_0, grow_1 = grow[:state_rows], grow[state_rows:]
-            crossed = pltpu.roll(jnp.where(even, grow_1, grow_0), HEAD_DIM, axis=1)
-            added = jnp.where(kept, jnp.where(even, grow_0, grow_1), crossed)
-            fade = dec_ref[at]
-            fade_turned = pltpu.roll(fade, HEAD_DIM, axis=1)
-            copies = state_rows // steps
-            factor = jnp.where(
-                kept,
-                jnp.concatenate([fade] * copies, axis=0),
-                jnp.concatenate([fade_turned] * copies, axis=0),
-            )
-            new_ref[slot, at] = factor * state + added
+            factor = jnp.concatenate([dec_ref[at]] * (state_rows // steps), axis=0)
+            new_ref[layer, chunk * seqs + at] = factor * state + grow
             return carry
 
         lax.fori_loop(0, seqs, one_sequence, 0, unroll=8)
@@ -730,14 +731,12 @@
         when(first & (chunk + 2 < chunks), relay_near, in_ref, in_sem, chunk + 2)
         when(slot == 0, relay_far, in_ref, in_sem, 1)
         state_load(slot).wait()
-        when(slot >= 2, lambda: state_store(slot - 2).wait())
-        advance(buffer)
+        advance(buffer, layer, chunk)
         when(mixed(5), relay_far, in_ref, in_sem, older(5) + chunks)
         when(slot >= 1, relay_near, y_ref, y_sem, older(1))
         when(first & (chunk + 2 < chunks), relay_far, in_ref, in_sem, chunk + 2)
         when(slot >= 2, relay_twin, y_ref, y_sem, older(2))
         read_out(item, layer)
-        state_store(slot).start()
         past, (past_layer, past_chunk) = older(3), place(slot - 3)
         when(slot >= 3, complete, y_ref, y_sem, past)
         begin(y_ref, y_sem, item, y_ref.at[item, me])
@@ -770,8 +769,6 @@
     finish(chunks - 4)
     sums_begin(chunks - 2)
     relay_twin(y_ref, y_sem, final)
-    state_store(items - 2).wait()
-    state_store(items - 1).wait()
     for item in range(items):
         drained(in_ref, in_sem, item)
         if item < final:
@@ -784,6 +781,42 @@
         finish(chunk)
     for chunk in range(chunks):
         sums_all(chunk).wait_send()
+
+
+def deliver_kernel(first_ref, second_ref, first_hbm, second_hbm, sem):
+    layers, parts = second_ref.shape[0], 4
+    size = second_ref.shape[1] // parts
+    copies = [pltpu.make_async_copy(first_ref, first_hbm, sem.at[layers * parts])]
+    for layer in range(layers):
+        for part in range(parts):
+            at = pl.ds(part * size, size)
+            copies.append(
+                pltpu.make_async_copy(
+                    second_ref.at[layer, at],
+                    second_hbm.at[layer, at],
+                    sem.at[layer * parts + part],
+                )
+            )
+    for copy in copies:
+        copy.start()
+    for copy in copies:
+        copy.wait()
+
+
+def deliver(first, second):
+    hbm = pl.BlockSpec(memory_space=pl.ANY)
+    return pl.pallas_call(
+        deliver_kernel,
+        out_shape=[
+            jax.ShapeDtypeStruct(first.shape, first.dtype),
+            jax.ShapeDtypeStruct(second.shape, second.dtype),
+        ],
+        in_specs=[hbm, hbm],
+        out_specs=[hbm, hbm],
+        scratch_shapes=[pltpu.SemaphoreType.DMA((4 * second.shape[0] + 1,))],
+        compiler_params=pltpu.CompilerParams(vmem_limit_bytes=1024 * 1024),
+        name="deliver",
+    )(first, second)
 
 
 def local_two_heads(
@@ -827,11 +860,11 @@
     current, new_memory = pl.pallas_call(
         lambda *refs: step_kernel(count, chunks, *refs),
         out_shape=[
-            jax.ShapeDtypeStruct((row_count, own_width), bf16),
-            jax.ShapeDtypeStruct(states.shape, f32),
+            pltpu.VMEM((row_count, own_width), bf16),
+            pltpu.VMEM(states.shape, f32),
         ],
         in_specs=[hbm] * 15,
-        out_specs=[vmem, hbm],
+        out_specs=[vmem, vmem],
         scratch_shapes=[
             pltpu.VMEM((2 * chunks, count, rows, own_width), bf16),
             pltpu.VMEM((2 * chunks, count, rows, LANES), bf16),
@@ -845,18 +878,17 @@
             pltpu.VMEM((chunks, count, 1, rows), f32),
             pltpu.VMEM((layers, batch_total, steps, LANES), f32),
             pltpu.VMEM(state_tile, f32),
-            pltpu.VMEM(state_tile, f32),
             pltpu.VMEM((rows, 5 * LANES), bf16),
             pltpu.VMEM(tile, f32),
             pltpu.VMEM((steps,) + tile, f32),
-            pltpu.VMEM((seqs, 2 * steps, LANES), bf16),
-            pltpu.VMEM((seqs, 2 * steps, LANES), bf16),
+            pltpu.VMEM((seqs, 8 * steps, LANES), bf16),
+            pltpu.VMEM((seqs, 8 * steps, LANES), bf16),
             pltpu.VMEM(tile, f32),
             pltpu.VMEM(tile, f32),
             pltpu.VMEM(tile, f32),
             pltpu.VMEM((2 * heads, 2 * LANES), bf16),
             pltpu.VMEM((2 * LANES, 2 * LANES), bf16),
-            pltpu.VMEM((LANES, LANES), bf16),
+            pltpu.VMEM((LANES, 4 * LANES), bf16),
             pltpu.VMEM((layers, steps, head_count, batch_total), f32),
             pltpu.VMEM((layers, features), f32),
             pltpu.VMEM((layers, features), f32),
@@ -864,14 +896,14 @@
             pltpu.SMEM((layers, head_count), f32),
             pltpu.SMEM((layers, head_count), f32),
             dma((20,)),
-            dma((2, 2)),
+            dma((2,)),
             dma((chunks,)),
             dma((3 + count // 4, 2 * chunks)),
             dma((3 + count // 4, 2 * chunks)),
             dma((2, chunks)),
         ],
         compiler_params=pltpu.CompilerParams(
-            collective_id=1, has_side_effects=True, vmem_limit_bytes=62 * 1024 * 1024
+            collective_id=1, has_side_effects=True, vmem_limit_bytes=46 * 1024 * 1024
         ),
         name="step",
     )(
@@ -891,6 +923,7 @@
         forgetting_magnitude_exponent,
         channel_forgetting_offset,
     )
+    current, new_memory = deliver(current, new_memory)
     new_memory = (
         new_memory.reshape(layers, batch_total, groups, head_count, LANES)
         .transpose(0, 1, 3, 2, 4)

time: 176 us -> 167 us (0.949)
  local copies, waits for them, and re-layouts: 9.24 us -> 0 us
    unnamed x2 -> x0, local copies, waits for them, and re-layouts: 9.24 us -> none
    pallas_call x0 -> x1, Pallas kernels: none -> 3.55 us  [deliver(): pl.pallas_call(deliver_kernel, out_shape=[jax.ShapeDtypeStruct(first.shap...]
    pallas_call x1, Pallas kernels: 165 us -> 162 us  [local_two_heads(): pl.pallas_call(lambda *refs: step_kernel(count, chunks, *refs), out_shape...]
where the time goes in v4:
time: 167 us; the launch traced here: 166 us
  Pallas kernels  166 us (99%)
    pallas_call x1, Pallas kernels, local_two_heads(): pl.pallas_call(lambda *refs: step_kernel(count, chunks, *refs), out_shape...  162 us
    pallas_call x1, Pallas kernels, deliver(): pl.pallas_call(deliver_kernel, out_shape=[jax.ShapeDtypeStruct(first.shap...  3.55 us

profile of v4, /device:TPU:0, one launch (start us, length us, event | category | flops | bytes accessed | tf_op | source)
XLA Modules:
  0.0 166.5 jit_solution(11211412379389679170)
XLA Ops:
  0.6 162.3 %step.1 = (bf16[1024,256]{1,0:T(8,128)(2,1)S(1)}, f32[2,128,64,128]{3,2,1,0:T(8,128)S(1)}) custom-call(bf16[1024,256]{1,0:T(8,128)(2,1)} %bitcast.16, bf16[2,4096,128]{2,1,0:T(8,128)(2,1)} %refs_1_.1, bf16[2,4096,128]{2,1,0:T(8,128)(2,1)} %refs_2_.1, bf16[2,4096,128]{2,1,0:T(8,128)(2,1)} %refs_3_.1, bf16[2,4096,128]{2,1,0:T(8,128)(2,1)} %refs_4_.1, ...), custom_call_target="tpu_custom_call" | custom-call | tf_op jit(solution)/shard_map/step/pallas_call | solution.py:860
  162.9 3.5 %deliver.1 = (bf16[1024,256]{1,0:T(8,128)(2,1)}, f32[2,128,64,128]{3,2,1,0:T(8,128)}) custom-call(bf16[1024,256]{1,0:T(8,128)(2,1)S(1)} %get-tuple-element.6.first_ref, f32[2,128,64,128]{3,2,1,0:T(8,128)S(1)} %get-tuple-element.7.second_ref), custom_call_target="tpu_custom_call" | custom-call | tf_op jit(solution)/shard_map/deliver/pallas_call | solution.py:808

commit v5 on v4

--- a/solution.py
+++ b/solution.py
@@ -243,7 +243,6 @@
 
 
 CHUNKS = 8
-AHEAD = 8
 GROUP_ROWS = 64
 
 
@@ -316,13 +315,25 @@
     own_heads = heads // count
 
     barrier = pltpu.get_barrier_semaphore()
-    for step in range(1, count):
+    inner = (line == 1) | (line == 2)
+    shifts = (0, 1 - 2 * lax.rem(line, 2), 2 - 4 * (line // 2), 3 - 2 * line)
+
+    def along(step):
+        return 4 * shifts[step]
+
+    def when(condition, action, *operands):
+        @pl.when(condition)
+        def _():
+            action(*operands)
+
+    def greet(device):
         pl.semaphore_signal(
-            barrier,
-            inc=1,
-            device_id={"tp": lax.rem(me + step, count)},
-            device_id_type=pl.DeviceIdType.MESH,
+            barrier, inc=1, device_id={"tp": device}, device_id_type=pl.DeviceIdType.MESH
         )
+
+    for device in (over, twin, me + along(1), me + along(2)):
+        greet(device)
+    when(inner, greet, me + along(3))
 
     loads = []
     for layer in range(2):
@@ -348,19 +359,8 @@
     for copy in loads:
         copy.start()
 
-    def place(slot):
-        past = slot - AHEAD
-        odd = lax.rem(past + 2 * AHEAD, 2)
-        layer = jnp.where(slot < AHEAD, 0, jnp.where(slot < items - AHEAD, 1 - odd, 1))
-        middle = jnp.where(slot < items - AHEAD, past // 2 + AHEAD * odd, slot - chunks)
-        return layer, jnp.where(slot < AHEAD, slot, middle)
-
-    def item_at(slot):
-        layer, chunk = place(slot)
-        return layer * chunks + chunk
-
     def state_load(slot):
-        layer, chunk = place(slot)
+        layer, chunk = slot // chunks, lax.rem(slot, chunks)
         return pltpu.make_async_copy(
             states_hbm.at[layer, pl.ds(chunk * seqs, seqs)],
             state_ref.at[lax.rem(slot, 2)],
@@ -369,7 +369,7 @@
 
     state_load(0).start()
 
-    pl.semaphore_wait(barrier, count - 1)
+    pl.semaphore_wait(barrier, 4 + lax.rem((line + 1) // 2, 2))
 
     def remote(source, target, send_sem, land_sem, device):
         return pltpu.make_async_remote_copy(
@@ -380,17 +380,6 @@
             device_id={"tp": device},
             device_id_type=pl.DeviceIdType.MESH,
         )
-
-    def when(condition, action, *operands):
-        @pl.when(condition)
-        def _():
-            action(*operands)
-
-    inner = (line == 1) | (line == 2)
-    shifts = (0, 1 - 2 * lax.rem(line, 2), 2 - 4 * (line // 2), 3 - 2 * line)
-
-    def along(step):
-        return 4 * shifts[step]
 
     def begin(buf, sems, item, source):
         target = buf.at[item, me]
@@ -456,8 +445,7 @@
         begin(in_ref, in_sem, item, x_hbm.at[pl.ds(item * rows, rows), :])
         own_copy(item).start()
 
-    for item in range(3):
-        begin_x(item)
+    begin_x(0)
 
     def iota(shape, axis):
         return lax.broadcasted_iota(jnp.int32, shape, axis)
@@ -487,12 +475,14 @@
         for origin in range(count):
             at = pl.ds(origin * width, width)
             pair = rates_ref[layer, :, at].astype(f32)
-            filled = jnp.concatenate([pair, jnp.zeros((LANES - 2 * heads, width), f32)], axis=0)
-            w_ref[layer, at, pl.ds(4 * LANES, LANES)] = filled.T.astype(bf16)
+            padded = jnp.concatenate([pair, jnp.zeros((LANES - 2 * heads, width), f32)], axis=0)
+            w_ref[layer, at, pl.ds(4 * LANES, LANES)] = padded.T.astype(bf16)
 
     relay_near(in_ref, in_sem, 0)
     relay_far(in_ref, in_sem, 0)
+    begin_x(1)
     relay_twin(in_ref, in_sem, 0)
+    begin_x(2)
 
     def squares(matrix):
         return matrix[:, :LANES] * matrix[:, :LANES] + matrix[:, LANES:] * matrix[:, LANES:]
@@ -699,84 +689,83 @@
             gain = post_gain_ref[1:2, pl.ds(pl.multiple_of(me * width + half * LANES, LANES), LANES)]
             before = xown_ref[chunk, :, at].astype(f32)
             mixed = mown_ref[chunk, :, at].astype(f32)
-            out_ref[pl.ds(chunk * rows, rows), at] = (before + mixed * scale * gain).astype(bf16)
+            out_ref[pl.ds(pl.multiple_of(chunk * rows, rows), rows), at] = (before + mixed * scale * gain).astype(bf16)
+
+    hold = chunks + 3
 
     def slot_of(slot, carry):
-        (layer, chunk), buffer = place(slot), lax.rem(slot, 2)
-        item = layer * chunks + chunk
-        first = layer == 0
+        layer, chunk, buffer = slot // chunks, lax.rem(slot, chunks), lax.rem(slot, 2)
+        busy, first = slot < items, slot < chunks
+
+        def early(by):
+            return (slot >= by) & (slot < by + chunks)
+
+        def late(by, action, *operands):
+            for side in (1, 0):
+                at = 2 * (slot - by - hold) - side
+                when((at >= 0) & (at < chunks), action, *operands, at + chunks)
+
         when(slot + 1 < items, lambda: state_load(slot + 1).start())
-        when(first & (chunk + 3 < chunks), lambda: begin_x(chunk + 3))
-        complete(in_ref, in_sem, item)
+        when(slot + 3 < chunks, lambda: begin_x(slot + 3))
+        when(busy, complete, in_ref, in_sem, slot)
 
         @pl.when(first)
         def _():
-            own_copy(chunk).wait()
-            first_hidden(chunk)
-
-        when(layer == 1, second_hidden, item)
-        proj_ref[...] = bf16_dot(h_ref[...], w_ref[layer]).astype(bf16)
-
-        def older(by):
-            return item_at(slot - by)
-
-        def mixed(by):
-            return (slot >= by) & (place(slot - by)[0] == 0)
-
-        when(mixed(5), relay_near, in_ref, in_sem, older(5) + chunks)
+            own_copy(slot).wait()
+            first_hidden(slot)
+
+        when(busy & (slot >= chunks), second_hidden, slot)
+
+        @pl.when(busy)
+        def _():
+            proj_ref[...] = bf16_dot(h_ref[...], w_ref[layer]).astype(bf16)
+
+        when(early(6), relay_far, in_ref, in_sem, slot - 6 + chunks)
         when(slot == 0, relay_near, in_ref, in_sem, 1)
-        when(slot >= 2, relay_far, y_ref, y_sem, older(2))
-        when(mixed(6), relay_twin, in_ref, in_sem, older(6) + chunks)
-        prepare(layer, chunk)
-        when(first & (chunk + 2 < chunks), relay_near, in_ref, in_sem, chunk + 2)
+        when(early(2), relay_far, y_ref, y_sem, slot - 2)
+        late(2, relay_far, y_ref, y_sem)
+        when(early(7), relay_twin, in_ref, in_sem, slot - 7 + chunks)
+        when(early(3), relay_twin, y_ref, y_sem, slot - 3)
+        late(3, relay_twin, y_ref, y_sem)
+        when(busy, prepare, layer, chunk)
+        when(slot + 2 < chunks, relay_near, in_ref, in_sem, slot + 2)
         when(slot == 0, relay_far, in_ref, in_sem, 1)
-        state_load(slot).wait()
-        advance(buffer, layer, chunk)
-        when(mixed(5), relay_far, in_ref, in_sem, older(5) + chunks)
-        when(slot >= 1, relay_near, y_ref, y_sem, older(1))
-        when(first & (chunk + 2 < chunks), relay_far, in_ref, in_sem, chunk + 2)
-        when(slot >= 2, relay_twin, y_ref, y_sem, older(2))
-        read_out(item, layer)
-        past, (past_layer, past_chunk) = older(3), place(slot - 3)
-        when(slot >= 3, complete, y_ref, y_sem, past)
-        begin(y_ref, y_sem, item, y_ref.at[item, me])
-        early = (slot >= 3) & (past_layer == 0)
-        late = (slot >= 3) & (past_layer == 1)
-        when(early, emit_middle, past)
-        when(late, emit_last, past)
-        when(first & (chunk + 1 < chunks), relay_twin, in_ref, in_sem, chunk + 1)
-
-        @pl.when(early)
+
+        @pl.when(busy)
         def _():
-            begin(in_ref, in_sem, past + chunks, in_ref.at[past + chunks, me])
-
-        when(late, sums_begin, past_chunk)
+            state_load(slot).wait()
+            advance(buffer, layer, chunk)
+
+        when(early(1), relay_near, y_ref, y_sem, slot - 1)
+        when(early(5), relay_near, in_ref, in_sem, slot - 5 + chunks)
+        late(1, relay_near, y_ref, y_sem)
+        when(slot + 2 < chunks, relay_far, in_ref, in_sem, slot + 2)
+        when(busy, read_out, slot, layer)
+        when(early(3), complete, y_ref, y_sem, slot - 3)
+        when(first, lambda: begin(y_ref, y_sem, slot, y_ref.at[slot, me]))
+        when(early(3), emit_middle, slot - 3)
+        late(3, complete, y_ref, y_sem)
+        late(3, emit_last)
+        when(slot + 1 < chunks, relay_twin, in_ref, in_sem, slot + 1)
+        late(0, lambda item: begin(y_ref, y_sem, item, y_ref.at[item, me]))
+
+        @pl.when(early(3))
+        def _():
+            made = slot - 3 + chunks
+            begin(in_ref, in_sem, made, in_ref.at[made, me])
+
+        late(3, lambda item: sums_begin(item - chunks))
+        late(5, lambda item: finish(item - chunks))
         return carry
 
-    lax.fori_loop(0, items, slot_of, 0)
-    final = items - 1
-    relay_far(y_ref, y_sem, final - 1)
-    complete(y_ref, y_sem, final - 2)
-    emit_last(final - 2)
-    relay_near(y_ref, y_sem, final)
-    relay_twin(y_ref, y_sem, final - 1)
-    sums_begin(chunks - 3)
-    for chunk in range(chunks - 4):
-        finish(chunk)
-    relay_far(y_ref, y_sem, final)
-    complete(y_ref, y_sem, final - 1)
-    emit_last(final - 1)
-    finish(chunks - 4)
-    sums_begin(chunks - 2)
-    relay_twin(y_ref, y_sem, final)
-    for item in range(items):
+    lax.fori_loop(0, items + 3, slot_of, 0)
+
+    def drain(item, carry):
         drained(in_ref, in_sem, item)
-        if item < final:
-            drained(y_ref, y_sem, item)
-    complete(y_ref, y_sem, final)
-    emit_last(final)
-    drained(y_ref, y_sem, final)
-    sums_begin(chunks - 1)
+        drained(y_ref, y_sem, item)
+        return carry
+
+    lax.fori_loop(0, items, drain, 0)
     for chunk in range(chunks - 3, chunks):
         finish(chunk)
     for chunk in range(chunks):

time: 167 us -> 151 us (0.904)
  Pallas kernels: 166 us -> 151 us
    pallas_call x1, Pallas kernels: 162 us -> 147 us  [local_two_heads(): pl.pallas_call(lambda *refs: step_kernel(count, chunks, *refs), out_shape...]
where the time goes in v5:
time: 151 us
  Pallas kernels  151 us (100%)
    pallas_call x1, Pallas kernels, local_two_heads(): pl.pallas_call(lambda *refs: step_kernel(count, chunks, *refs), out_shape...  147 us
    pallas_call x1, Pallas kernels, deliver(): pl.pallas_call(deliver_kernel, out_shape=[jax.ShapeDtypeStruct(first.shap...  3.55 us

profile of v5, /device:TPU:0, one launch (start us, length us, event | category | flops | bytes accessed | tf_op | source)
XLA Modules:
  0.0 151.3 jit_solution(87973179554357930)
XLA Ops:
  0.6 147.1 %step.1 = (bf16[1024,256]{1,0:T(8,128)(2,1)S(1)}, f32[2,128,64,128]{3,2,1,0:T(8,128)S(1)}) custom-call(bf16[1024,256]{1,0:T(8,128)(2,1)} %bitcast.16, bf16[2,4096,128]{2,1,0:T(8,128)(2,1)} %refs_1_.1, bf16[2,4096,128]{2,1,0:T(8,128)(2,1)} %refs_2_.1, bf16[2,4096,128]{2,1,0:T(8,128)(2,1)} %refs_3_.1, bf16[2,4096,128]{2,1,0:T(8,128)(2,1)} %refs_4_.1, ...), custom_call_target="tpu_custom_call" | custom-call | tf_op jit(solution)/shard_map/step/pallas_call | solution.py:849
  147.8 3.5 %deliver.1 = (bf16[1024,256]{1,0:T(8,128)(2,1)}, f32[2,128,64,128]{3,2,1,0:T(8,128)}) custom-call(bf16[1024,256]{1,0:T(8,128)(2,1)S(1)} %get-tuple-element.6.first_ref, f32[2,128,64,128]{3,2,1,0:T(8,128)S(1)} %get-tuple-element.7.second_ref), custom_call_target="tpu_custom_call" | custom-call | tf_op jit(solution)/shard_map/deliver/pallas_call | solution.py:797

commit v6 on v5

--- a/solution.py
+++ b/solution.py
@@ -381,6 +381,9 @@
             device_id_type=pl.DeviceIdType.MESH,
         )
 
+    def plain(buf, item):
+        return (item == items - 1) if buf is y_ref else (item < 0)
+
     def begin(buf, sems, item, source):
         target = buf.at[item, me]
 
@@ -389,7 +392,7 @@
 
         out(5, me + along(2))
         out(4, me + along(1))
-        when(inner, out, 6, me + along(3))
+        when(inner | (plain(buf, item)), out, 6, me + along(3))
         out(1, over)
         out(3, twin)
 
@@ -405,7 +408,8 @@
 
     def relay_near(buf, sems, item):
         landed(buf, sems, item, 5, 1)
-        when(inner, pass_on, buf, sems, item, me + along(2), 6, me + along(1))
+        onward = inner & jnp.logical_not(plain(buf, item))
+        when(onward, pass_on, buf, sems, item, me + along(2), 6, me + along(1))
         pass_on(buf, sems, item, me + along(2), 2, over)
         pass_on(buf, sems, item, me + along(2), 3, twin)
         landed(buf, sems, item, 1, 1)
@@ -433,8 +437,10 @@
             part = buf.at[item, pl.ds(0, blocks)]
             remote(part, part, sems.at[0, item], sems.at[1, item], twin).wait_send()
 
-        when(inner, sent, count)
-        when(jnp.logical_not(inner), sent, count - 2)
+        last = plain(buf, item)
+        when(last, sent, count - 1)
+        when(inner & jnp.logical_not(last), sent, count)
+        when(jnp.logical_not(inner | last), sent, count - 2)
 
     def own_copy(item):
         return pltpu.make_async_copy(
@@ -483,6 +489,7 @@
     begin_x(1)
     relay_twin(in_ref, in_sem, 0)
     begin_x(2)
+    begin_x(3)
 
     def squares(matrix):
         return matrix[:, :LANES] * matrix[:, :LANES] + matrix[:, LANES:] * matrix[:, LANES:]
@@ -706,7 +713,7 @@
                 when((at >= 0) & (at < chunks), action, *operands, at + chunks)
 
         when(slot + 1 < items, lambda: state_load(slot + 1).start())
-        when(slot + 3 < chunks, lambda: begin_x(slot + 3))
+        when(slot + 4 < chunks, lambda: begin_x(slot + 4))
         when(busy, complete, in_ref, in_sem, slot)
 
         @pl.when(first)
@@ -755,10 +762,34 @@
             begin(in_ref, in_sem, made, in_ref.at[made, me])
 
         late(3, lambda item: sums_begin(item - chunks))
-        late(5, lambda item: finish(item - chunks))
         return carry
 
-    lax.fori_loop(0, items + 3, slot_of, 0)
+    lax.fori_loop(0, items, slot_of, 0)
+    final = items - 1
+
+    def emit_pair(*targets):
+        for target in targets:
+            complete(y_ref, y_sem, target)
+            emit_last(target)
+        for target in targets:
+            sums_begin(target - chunks)
+
+    for target in (final - 2, final - 1):
+        relay_far(y_ref, y_sem, target)
+    for target in (final - 4, final - 3):
+        relay_twin(y_ref, y_sem, target)
+    relay_near(y_ref, y_sem, final)
+    relay_far(y_ref, y_sem, final)
+    emit_pair(final - 4, final - 3)
+    for target in (final - 2, final - 1):
+        relay_twin(y_ref, y_sem, target)
+    for chunk in range(3):
+        finish(chunk)
+    emit_pair(final - 2, final - 1)
+    relay_twin(y_ref, y_sem, final)
+    for chunk in range(3, 5):
+        finish(chunk)
+    emit_pair(final)
 
     def drain(item, carry):
         drained(in_ref, in_sem, item)
@@ -773,7 +804,7 @@
 
 
 def deliver_kernel(first_ref, second_ref, first_hbm, second_hbm, sem):
-    layers, parts = second_ref.shape[0], 4
+    layers, parts = second_ref.shape[0], 16
     size = second_ref.shape[1] // parts
     copies = [pltpu.make_async_copy(first_ref, first_hbm, sem.at[layers * parts])]
     for layer in range(layers):
@@ -802,7 +833,7 @@
         ],
         in_specs=[hbm, hbm],
         out_specs=[hbm, hbm],
-        scratch_shapes=[pltpu.SemaphoreType.DMA((4 * second.shape[0] + 1,))],
+        scratch_shapes=[pltpu.SemaphoreType.DMA((16 * second.shape[0] + 1,))],
         compiler_params=pltpu.CompilerParams(vmem_limit_bytes=1024 * 1024),
         name="deliver",
     )(first, second)

time: 151 us -> 149 us (0.987)
  Pallas kernels: 151 us -> 148 us
    pallas_call x1, Pallas kernels: 147 us -> 145 us  [local_two_heads(): pl.pallas_call(lambda *refs: step_kernel(count, chunks, *refs), out_shape...]
where the time goes in v6:
time: 149 us
  Pallas kernels  148 us (99%)
    pallas_call x1, Pallas kernels, local_two_heads(): pl.pallas_call(lambda *refs: step_kernel(count, chunks, *refs), out_shape...  145 us
    pallas_call x1, Pallas kernels, deliver(): pl.pallas_call(deliver_kernel, out_shape=[jax.ShapeDtypeStruct(first.shap...  3.71 us

profile of v6, /device:TPU:0, one launch (start us, length us, event | category | flops | bytes accessed | tf_op | source)
XLA Modules:
  0.0 149.1 jit_solution(9902081641690057620)
XLA Ops:
  0.6 144.7 %step.1 = (bf16[1024,256]{1,0:T(8,128)(2,1)S(1)}, f32[2,128,64,128]{3,2,1,0:T(8,128)S(1)}) custom-call(bf16[1024,256]{1,0:T(8,128)(2,1)} %bitcast.16, bf16[2,4096,128]{2,1,0:T(8,128)(2,1)} %refs_1_.1, bf16[2,4096,128]{2,1,0:T(8,128)(2,1)} %refs_2_.1, bf16[2,4096,128]{2,1,0:T(8,128)(2,1)} %refs_3_.1, bf16[2,4096,128]{2,1,0:T(8,128)(2,1)} %refs_4_.1, ...), custom_call_target="tpu_custom_call" | custom-call | tf_op jit(solution)/shard_map/step/pallas_call | solution.py:880
  145.3 3.7 %deliver.1 = (bf16[1024,256]{1,0:T(8,128)(2,1)}, f32[2,128,64,128]{3,2,1,0:T(8,128)}) custom-call(bf16[1024,256]{1,0:T(8,128)(2,1)S(1)} %get-tuple-element.6.first_ref, f32[2,128,64,128]{3,2,1,0:T(8,128)S(1)} %get-tuple-element.7.second_ref), custom_call_target="tpu_custom_call" | custom-call | tf_op jit(solution)/shard_map/deliver/pallas_call | solution.py:828
